TPU v7x, 32 devices: a whole 2x2x4 slice. The times are simulated.
32 devices in a mesh: sp: 8 (over z, x), tp: 4 (over y, core).
Axes of the slice: x: 2, y: 2, z: 4, core: 2. Of those that a mesh axis runs over, the one named last changes fastest.
Arguments:
- inputs: bfloat16 [8192, 2048], P('sp'), may hold values from -9 to 9
- w_query: bfloat16 [2048, 1024], P(None, 'tp'), may hold values from -0.15692044 to 0.15692044
- w_key: bfloat16 [2048, 1024], P(None, 'tp'), may hold values from -0.15692044 to 0.15692044
- w_value: bfloat16 [2048, 1024], P(None, 'tp'), may hold values from -0.125 to 0.125
- w_glu_value: bfloat16 [2048, 1024], P(None, 'tp'), may hold values from -0.37565048 to 0.37565048
- w_glu_gate: bfloat16 [2048, 1024], P(None, 'tp'), may hold values from -0.125 to 0.125
- conv_taps: float32 [31, 1024], P(None, 'tp'), may hold values from -4 to 4
- conv_gain: float32 [1024], P('tp'), may hold values from 0.1 to 1.9
- log_forget: float32 [8192, 8], P('sp', 'tp'), may hold values from -8192 to 0, as said below
- w_out: bfloat16 [2048, 2048], replicated, may hold values from -0.125 to 0.125
Outputs:
- result: bfloat16 [8192, 2048], P(('sp', 'tp'))
Inputs may be any that keep to these rules, and one draw needn't show every extreme that they name: `log_forget`: for each head, non-increasing along positions and at most zero.
All inputs are finite; a program needn't handle non-finite values.
Results may differ from a plain program's by a relative error of at most 0.014.
Values may be sent and summed in bfloat16 or wider, within the bound.
A program may use at most 128 MiB of HBM per device.

v0:
```python
import math

import jax
import jax.numpy as jnp
from jax import lax
from jax.sharding import PartitionSpec as P

HEAD_DIM = 128


NORM_EPS = 1e-05


def passed_along(value, axis, steps):
    count = lax.axis_size(axis)
    leading, last = (max(0, -steps), min(count, count - steps))
    return lax.ppermute(value, axis, [(source, source + steps) for source in range(leading, last)])


def on_device(
    inputs,
    w_query,
    w_key,
    w_value,
    w_glu_value,
    w_glu_gate,
    conv_taps,
    conv_gain,
    log_forget,
    w_out,
):
    tok_rows = inputs.shape[0]
    channels = w_glu_value.shape[1]
    heads_here = w_query.shape[1] // HEAD_DIM
    attn_width = heads_here * HEAD_DIM
    tp_count = lax.axis_size("tp")
    tp_place = lax.axis_index("tp")
    total_channels = channels * tp_count
    row_start = lax.axis_index("sp") * tok_rows
    last_row = row_start + tok_rows - 1
    glu_value = jnp.dot(inputs, w_glu_value, preferred_element_type=jnp.float32)
    glu_gate = jnp.dot(inputs, w_glu_gate, preferred_element_type=jnp.float32)
    gated = (glu_value * jax.nn.sigmoid(glu_gate)).astype(jnp.bfloat16)
    kernel = conv_taps.shape[0]
    halo_rows = passed_along(gated[tok_rows - (kernel - 1) :], "sp", 1)
    padded = jnp.concatenate([halo_rows, gated], axis=0).astype(jnp.float32)
    conv_sum = jnp.zeros((tok_rows, channels), jnp.float32)
    for offset in range(kernel):
        conv_sum = conv_sum + conv_taps[offset] * padded[offset : offset + tok_rows]
    mean_value = lax.psum(jnp.sum(conv_sum, axis=1), "tp") / total_channels
    centered = conv_sum - mean_value[:, None]
    spread = lax.psum(jnp.sum(centered * centered, axis=1), "tp") / total_channels
    conv_rows = jax.nn.silu(centered * lax.rsqrt(spread + NORM_EPS)[:, None] * conv_gain).astype(
        jnp.bfloat16
    )
    query_rows = jnp.dot(inputs, w_query, preferred_element_type=jnp.float32).astype(jnp.bfloat16)
    key_rows = jnp.dot(inputs, w_key, preferred_element_type=jnp.float32).astype(jnp.bfloat16)
    value_rows = jnp.dot(inputs, w_value, preferred_element_type=jnp.float32).astype(jnp.bfloat16)
    query_heads = query_rows.reshape(tok_rows, heads_here, HEAD_DIM)
    own_gates = jnp.transpose(log_forget)
    gates_all = lax.all_gather(log_forget, "sp", axis=0, tiled=True)
    score_scale = HEAD_DIM ** (-0.5)
    query_pos = row_start + jnp.arange(tok_rows, dtype=jnp.int32)
    start_state = (
        jnp.full((heads_here, tok_rows), -1e30, jnp.float32),
        jnp.zeros((heads_here, tok_rows), jnp.float32),
        jnp.zeros((heads_here, tok_rows, HEAD_DIM), jnp.float32),
    )
    piece_keys = lax.all_gather(key_rows, "sp", axis=0, tiled=True)
    piece_values = lax.all_gather(value_rows, "sp", axis=0, tiled=True)
    block_rows = math.gcd(piece_keys.shape[0], tok_rows)
    shards = piece_keys.shape[0] // block_rows
    key_iota = jnp.arange(block_rows, dtype=jnp.int32)

    def one_shard(shard_number, carried_state):
        offset = shard_number * block_rows
        key_first = offset

        def attend(state_in):
            running_max, running_sum, running_out = state_in
            shard_keys = lax.dynamic_slice_in_dim(piece_keys, offset, block_rows, 0).reshape(
                block_rows, heads_here, HEAD_DIM
            )
            shard_values = lax.dynamic_slice_in_dim(piece_values, offset, block_rows, 0).reshape(
                block_rows, heads_here, HEAD_DIM
            )
            shard_gates = jnp.transpose(
                lax.dynamic_slice_in_dim(gates_all, key_first, block_rows, 0)
            )
            scores = (
                jnp.einsum(
                    "qhd,khd->hqk", query_heads, shard_keys, preferred_element_type=jnp.float32
                )
                * score_scale
            )
            scores = scores + own_gates[:, :, None] - shard_gates[:, None, :]
            allowed = ((key_first + key_iota)[None, :] <= query_pos[:, None])[None]
            masked = jnp.where(allowed, scores, -1e30)
            new_max = jnp.maximum(running_max, jnp.max(masked, axis=2))
            weights = jnp.where(allowed, jnp.exp(masked - new_max[:, :, None]), 0.0)
            rescale = jnp.exp(running_max - new_max)
            new_sum = running_sum * rescale + jnp.sum(weights, axis=2)
            mixture = jnp.einsum(
                "hqk,khd->hqd",
                weights.astype(jnp.bfloat16),
                shard_values,
                preferred_element_type=jnp.float32,
            )
            new_out = running_out * rescale[:, :, None] + mixture
            return (new_max, new_sum, new_out)

        def keep_state(state_in):
            return state_in

        return lax.cond(key_first <= last_row, attend, keep_state, carried_state)

    final_max, final_sum, final_out = lax.fori_loop(0, shards, one_shard, start_state)
    attn_heads = (final_out / final_sum[:, :, None]).astype(jnp.bfloat16)
    attn_rows = jnp.transpose(attn_heads, (1, 0, 2)).reshape(tok_rows, attn_width)
    conv_weight = lax.dynamic_slice_in_dim(w_out, tp_place * channels, channels, 0)
    attn_weight = lax.dynamic_slice_in_dim(
        w_out, total_channels + tp_place * attn_width, attn_width, 0
    )
    projected = jnp.dot(conv_rows, conv_weight, preferred_element_type=jnp.float32)
    return lax.psum_scatter(
        (projected + jnp.dot(attn_rows, attn_weight, preferred_element_type=jnp.float32)).astype(
            jnp.bfloat16
        ),
        "tp",
        scatter_dimension=0,
        tiled=True,
    )


def solution(mesh):
    in_specs = (
        P("sp", None),
        P(None, "tp"),
        P(None, "tp"),
        P(None, "tp"),
        P(None, "tp"),
        P(None, "tp"),
        P(None, "tp"),
        P("tp"),
        P("sp", "tp"),
        P(),
    )
    out_specs = P(("sp", "tp"), None)
    return jax.shard_map(
        on_device, mesh=mesh, in_specs=in_specs, out_specs=out_specs, check_vma=False
    )
```

profile of v0, /device:TPU:24, one launch (start us, length us, event | category | flops | bytes accessed | tf_op | source)
XLA Modules:
  0.0 320.0 jit_solution(7589455608530308768)
XLA Ops:
  7.8 4.2 %convolution_convert_fusion.2 = bf16[1024,256]{1,0:T(8,128)(2,1)} fusion(bf16[1024,2048]{1,0:T(8,128)(2,1)} %param.14, bf16[2048,256]{1,0:T(8,128)(2,1)S(1)} %copy-done), kind=kOutput, calls=%fused_computation.30 | convolution fusion | flops 1074003968 | bytes 5767168 | tf_op jit(solution)/shard_map/dot_general | solution.py:57
  12.1 4.6 %convolution_convert_fusion = bf16[1024,256]{1,0:T(8,128)(2,1)} fusion(bf16[1024,2048]{1,0:T(8,128)(2,1)} %param.14, bf16[2048,256]{1,0:T(8,128)(2,1)} %param.17), kind=kOutput, calls=%fused_computation.28 | convolution fusion | flops 1074003968 | bytes 5767168 | tf_op jit(solution)/shard_map/dot_general | solution.py:58
  16.8 3.6 %fusion.18 = f32[1024,256]{1,0:T(8,128)S(1)} fusion(bf16[1024,2048]{1,0:T(8,128)(2,1)} %param.14, bf16[2048,256]{1,0:T(8,128)(2,1)S(1)} %copy-done.6), kind=kOutput, calls=%fused_computation.26 | convolution fusion | flops 1074528256 | bytes 6291456 | tf_op jit(solution)/shard_map/dot_general | solution.py:42
  21.7 3.4 %collective-permute-start = (bf16[30,256]{1,0:T(8,128)(2,1)S(1)}, bf16[30,256]{1,0:T(8,128)(2,1)S(1)}, u32[]{:S(2)}, u32[]{:S(2)}) collective-permute-start(bf16[30,256]{1,0:T(8,128)(2,1)S(1)} %slice.252), channel_id=1, source_target_pairs={{0,4},{4,8},{8,12},{12,16},{16,20},{20,24},{24,28},{1,5},{5,9},{9,... | collective-permute-start | bytes 46088 | tf_op jit(solution)/shard_map/ppermute | solution.py:17
  25.1 3.8 %convolution_convert_fusion.1 = bf16[1024,256]{0,1:T(8,128)(2,1)S(1)} fusion(bf16[1024,2048]{1,0:T(8,128)(2,1)} %param.14, bf16[2048,256]{1,0:T(8,128)(2,1)} %param.15), kind=kOutput, calls=%fused_computation.29 | convolution fusion | flops 1074003968 | bytes 5767168 | tf_op jit(solution)/shard_map/dot_general | solution.py:56
  29.3 28.8 %all_gather.10 = f32[8192,2]{0,1:T(2,128)S(1)} all-gather(f32[1024,2]{0,1:T(2,128)S(1)} %copy-done.2), channel_id=1, replica_groups=mesh['sp'=8,'tp'=4] {'sp'}, dimensions={0}, use_global_device_ids=true | all-gather | bytes 73728 | tf_op jit(solution)/shard_map/all_gather | solution.py:61
  58.2 4.3 %fusion.60 = (f32[1024]{0:T(1024)S(1)}, f32[1024,256]{1,0:T(8,128)S(1)}) fusion(f32[1054,256]{1,0:T(8,128)S(1)} %maximum_convert_fusion, f32[256]{0:T(256)S(1)} %bitcast.80, f32[256]{0:T(256)S(1)} %bitcast.81, f32[256]{0:T(256)S(1)} %bitcast.83, f32[256]{0:T(256)S(1)} %bitcast.84, f32[256]{0:T(256)S(1)} %bitcast.85, f32[256]{0:T(256)S(1)} %bitcast.86, ...), kind=kLoop, calls=%fused_computation.108 | loop fusion | flops 16251904 | bytes 33590272 | tf_op jit(solution)/shard_map/reduce_sum | solution.py:50
  62.5 6.1 %psum.14 = f32[1024]{0:T(1024)S(1)} all-reduce(f32[1024]{0:T(1024)S(1)} %get-tuple-element.333), channel_id=1, replica_groups=mesh['sp'=8,'tp'=4] {'tp'}, use_global_device_ids=true, to_apply=%region_1.0 | all-reduce | flops 1024 | bytes 8192 | tf_op jit(solution)/shard_map/psum | solution.py:50
  69.0 6.2 %psum.15 = f32[1024]{0:T(1024)S(1)} all-reduce(f32[1024]{0:T(1024)S(1)} %multiply_reduce_fusion), channel_id=1, replica_groups=mesh['sp'=8,'tp'=4] {'tp'}, use_global_device_ids=true, to_apply=%region_3.0 | all-reduce | flops 1024 | bytes 8192 | tf_op jit(solution)/shard_map/psum | solution.py:52
  75.2 5.8 %fusion.51 = f32[1024,2048]{1,0:T(8,128)} fusion(bf16[2048,2048]{1,0:T(8,128)(2,1)} %param.23, s32[]{:T(128)S(6)} %select_n.18, f32[1024,256]{1,0:T(8,128)S(1)} %get-tuple-element.334, f32[256]{0:T(256)S(1)} %copy-done.4, f32[1024]{0:T(1024)S(1)} %add_rsqrt_fusion, f32[1024]{0:T(1024)S(1)} %broadcast_multiply_fusion), kind=kOutput, calls=%fused_computation.94 | convolution fusion | flops 1075838976 | bytes 10494980 | tf_op jit(solution)/shard_map/dot_general | solution.py:124
  81.0 4.3 %all-gather.3.cloned.1.call-done = bf16[8192,256]{1,0:T(8,128)(2,1)} async-done(((bf16[1024,256]{1,0:T(8,128)(2,1)}), bf16[8192,256]{1,0:T(8,128)(2,1)}) %all-gather.3.cloned.1.call-update) | async-done | bytes 4194320 | tf_op jit(solution)/shard_map/all_gather | solution.py:69
  85.3 6.4 %copy.16 = bf16[8192,256]{0,1:T(8,128)(2,1)} copy(bf16[8192,256]{1,0:T(8,128)(2,1)} %all-gather.3.cloned.1.call-done) | data formatting | bytes 8388608
  91.8 67.1 %all-gather.5.cloned.1.call-done = bf16[8192,256]{1,0:T(8,128)(2,1)} async-done(((bf16[1024,256]{1,0:T(8,128)(2,1)}), bf16[8192,256]{1,0:T(8,128)(2,1)}) %all-gather.5.cloned.1.call-update) | async-done | bytes 4194320 | tf_op jit(solution)/shard_map/all_gather | solution.py:70
  158.9 6.4 %copy.18 = bf16[8192,256]{0,1:T(8,128)(2,1)} copy(bf16[8192,256]{1,0:T(8,128)(2,1)} %all-gather.5.cloned.1.call-done) | data formatting | bytes 8388608
  165.4 83.9 %while.18 = (s32[]{:T(128)}, f32[2,1024]{1,0:T(2,128)S(1)}, f32[2,1024]{1,0:T(2,128)S(1)}, f32[2,1024,128]{2,1,0:T(8,128)S(1)}, s32[]{:T(128)}, /*index=5*/bf16[...) while((s32[]{:T(128)}, f32[2,1024]{1,0:T(2,128)S(1)}, ...), condition=%wide.region_9.10_spmd.clone, body=%wide.region_4.9_spmd.clone.sunk | while | flops 1115166720 | bytes 35352928 | solution.py:117
  165.4 11.9 %conditional.3 = ((f32[2,1024]{1,0:T(2,128)S(1)}, f32[2,1024]{1,0:T(2,128)S(1)}, f32[2,1024,128]{2,1,0:T(8,128)S(1)})) conditional(s32[]{:T(128)} %convert_element_type.57, (f32[2,1024]{1,0:T(2,128)S(1)}, f32[2,1024]{1,0:T(2,128)S(1)}, f32[2,1024,128]{2,1,0:T(8,128)S(1)}) %tuple.78, (s32[]{:T(128)}, s32[1024]{0:T(1024)S(1)}, s32[]{:T(128)}, ...), branch_computations={%region_5.5_spmd, %region_6.8_spmd} | conditional | flops 1115166720 | bytes 35348560 | solution.py:115
  170.1 3.0 fusion.5
  173.1 4.2 %fusion.10 = f32[2,1024,128]{2,1,0:T(8,128)S(1)} fusion(bf16[1024,2,128]{0,2,1:T(8,128)(2,1)S(1)} %bitcast.65, f32[2,1024,1024]{2,1,0:T(8,128)S(1)} %get-tuple-element.336, f32[2,1024]{1,0:T(2,128)S(1)} %max.2, f32[2,1024]{1,0:T(2,128)S(1)} %dynamic-slice_bitcast_fusion, f32[2,1024]{1,0:T(2,128)S(1)} %get-tuple-element.230, ...), kind=kOutput, calls=%fused_computation.10 | convolution fusion | flops 552075264 | bytes 12091392 | tf_op jit(solution)/shard_map/while/body/eval_jaxpr/cond/branch_1_fun/hqk,khd->hqd/dot_general | solution.py:103
  177.4 11.9 %conditional.3 = ((f32[2,1024]{1,0:T(2,128)S(1)}, f32[2,1024]{1,0:T(2,128)S(1)}, f32[2,1024,128]{2,1,0:T(8,128)S(1)})) conditional(s32[]{:T(128)} %convert_element_type.57, (f32[2,1024]{1,0:T(2,128)S(1)}, f32[2,1024]{1,0:T(2,128)S(1)}, f32[2,1024,128]{2,1,0:T(8,128)S(1)}) %tuple.78, (s32[]{:T(128)}, s32[1024]{0:T(1024)S(1)}, s32[]{:T(128)}, ...), branch_computations={%region_5.5_spmd, %region_6.8_spmd} | conditional | flops 1115166720 | bytes 35348560 | solution.py:115
  185.1 4.2 %fusion.10 = f32[2,1024,128]{2,1,0:T(8,128)S(1)} fusion(bf16[1024,2,128]{0,2,1:T(8,128)(2,1)S(1)} %bitcast.65, f32[2,1024,1024]{2,1,0:T(8,128)S(1)} %get-tuple-element.336, f32[2,1024]{1,0:T(2,128)S(1)} %max.2, f32[2,1024]{1,0:T(2,128)S(1)} %dynamic-slice_bitcast_fusion, f32[2,1024]{1,0:T(2,128)S(1)} %get-tuple-element.230, ...), kind=kOutput, calls=%fused_computation.10 | convolution fusion | flops 552075264 | bytes 12091392 | tf_op jit(solution)/shard_map/while/body/eval_jaxpr/cond/branch_1_fun/hqk,khd->hqd/dot_general | solution.py:103
  189.4 11.9 %conditional.3 = ((f32[2,1024]{1,0:T(2,128)S(1)}, f32[2,1024]{1,0:T(2,128)S(1)}, f32[2,1024,128]{2,1,0:T(8,128)S(1)})) conditional(s32[]{:T(128)} %convert_element_type.57, (f32[2,1024]{1,0:T(2,128)S(1)}, f32[2,1024]{1,0:T(2,128)S(1)}, f32[2,1024,128]{2,1,0:T(8,128)S(1)}) %tuple.78, (s32[]{:T(128)}, s32[1024]{0:T(1024)S(1)}, s32[]{:T(128)}, ...), branch_computations={%region_5.5_spmd, %region_6.8_spmd} | conditional | flops 1115166720 | bytes 35348560 | solution.py:115
  197.1 4.2 %fusion.10 = f32[2,1024,128]{2,1,0:T(8,128)S(1)} fusion(bf16[1024,2,128]{0,2,1:T(8,128)(2,1)S(1)} %bitcast.65, f32[2,1024,1024]{2,1,0:T(8,128)S(1)} %get-tuple-element.336, f32[2,1024]{1,0:T(2,128)S(1)} %max.2, f32[2,1024]{1,0:T(2,128)S(1)} %dynamic-slice_bitcast_fusion, f32[2,1024]{1,0:T(2,128)S(1)} %get-tuple-element.230, ...), kind=kOutput, calls=%fused_computation.10 | convolution fusion | flops 552075264 | bytes 12091392 | tf_op jit(solution)/shard_map/while/body/eval_jaxpr/cond/branch_1_fun/hqk,khd->hqd/dot_general | solution.py:103
  201.3 11.9 %conditional.3 = ((f32[2,1024]{1,0:T(2,128)S(1)}, f32[2,1024]{1,0:T(2,128)S(1)}, f32[2,1024,128]{2,1,0:T(8,128)S(1)})) conditional(s32[]{:T(128)} %convert_element_type.57, (f32[2,1024]{1,0:T(2,128)S(1)}, f32[2,1024]{1,0:T(2,128)S(1)}, f32[2,1024,128]{2,1,0:T(8,128)S(1)}) %tuple.78, (s32[]{:T(128)}, s32[1024]{0:T(1024)S(1)}, s32[]{:T(128)}, ...), branch_computations={%region_5.5_spmd, %region_6.8_spmd} | conditional | flops 1115166720 | bytes 35348560 | solution.py:115
  209.0 4.2 %fusion.10 = f32[2,1024,128]{2,1,0:T(8,128)S(1)} fusion(bf16[1024,2,128]{0,2,1:T(8,128)(2,1)S(1)} %bitcast.65, f32[2,1024,1024]{2,1,0:T(8,128)S(1)} %get-tuple-element.336, f32[2,1024]{1,0:T(2,128)S(1)} %max.2, f32[2,1024]{1,0:T(2,128)S(1)} %dynamic-slice_bitcast_fusion, f32[2,1024]{1,0:T(2,128)S(1)} %get-tuple-element.230, ...), kind=kOutput, calls=%fused_computation.10 | convolution fusion | flops 552075264 | bytes 12091392 | tf_op jit(solution)/shard_map/while/body/eval_jaxpr/cond/branch_1_fun/hqk,khd->hqd/dot_general | solution.py:103
  213.3 11.9 %conditional.3 = ((f32[2,1024]{1,0:T(2,128)S(1)}, f32[2,1024]{1,0:T(2,128)S(1)}, f32[2,1024,128]{2,1,0:T(8,128)S(1)})) conditional(s32[]{:T(128)} %convert_element_type.57, (f32[2,1024]{1,0:T(2,128)S(1)}, f32[2,1024]{1,0:T(2,128)S(1)}, f32[2,1024,128]{2,1,0:T(8,128)S(1)}) %tuple.78, (s32[]{:T(128)}, s32[1024]{0:T(1024)S(1)}, s32[]{:T(128)}, ...), branch_computations={%region_5.5_spmd, %region_6.8_spmd} | conditional | flops 1115166720 | bytes 35348560 | solution.py:115
  221.0 4.2 %fusion.10 = f32[2,1024,128]{2,1,0:T(8,128)S(1)} fusion(bf16[1024,2,128]{0,2,1:T(8,128)(2,1)S(1)} %bitcast.65, f32[2,1024,1024]{2,1,0:T(8,128)S(1)} %get-tuple-element.336, f32[2,1024]{1,0:T(2,128)S(1)} %max.2, f32[2,1024]{1,0:T(2,128)S(1)} %dynamic-slice_bitcast_fusion, f32[2,1024]{1,0:T(2,128)S(1)} %get-tuple-element.230, ...), kind=kOutput, calls=%fused_computation.10 | convolution fusion | flops 552075264 | bytes 12091392 | tf_op jit(solution)/shard_map/while/body/eval_jaxpr/cond/branch_1_fun/hqk,khd->hqd/dot_general | solution.py:103
  225.3 11.9 %conditional.3 = ((f32[2,1024]{1,0:T(2,128)S(1)}, f32[2,1024]{1,0:T(2,128)S(1)}, f32[2,1024,128]{2,1,0:T(8,128)S(1)})) conditional(s32[]{:T(128)} %convert_element_type.57, (f32[2,1024]{1,0:T(2,128)S(1)}, f32[2,1024]{1,0:T(2,128)S(1)}, f32[2,1024,128]{2,1,0:T(8,128)S(1)}) %tuple.78, (s32[]{:T(128)}, s32[1024]{0:T(1024)S(1)}, s32[]{:T(128)}, ...), branch_computations={%region_5.5_spmd, %region_6.8_spmd} | conditional | flops 1115166720 | bytes 35348560 | solution.py:115
  233.0 4.2 %fusion.10 = f32[2,1024,128]{2,1,0:T(8,128)S(1)} fusion(bf16[1024,2,128]{0,2,1:T(8,128)(2,1)S(1)} %bitcast.65, f32[2,1024,1024]{2,1,0:T(8,128)S(1)} %get-tuple-element.336, f32[2,1024]{1,0:T(2,128)S(1)} %max.2, f32[2,1024]{1,0:T(2,128)S(1)} %dynamic-slice_bitcast_fusion, f32[2,1024]{1,0:T(2,128)S(1)} %get-tuple-element.230, ...), kind=kOutput, calls=%fused_computation.10 | convolution fusion | flops 552075264 | bytes 12091392 | tf_op jit(solution)/shard_map/while/body/eval_jaxpr/cond/branch_1_fun/hqk,khd->hqd/dot_general | solution.py:103
  237.3 11.9 %conditional.3 = ((f32[2,1024]{1,0:T(2,128)S(1)}, f32[2,1024]{1,0:T(2,128)S(1)}, f32[2,1024,128]{2,1,0:T(8,128)S(1)})) conditional(s32[]{:T(128)} %convert_element_type.57, (f32[2,1024]{1,0:T(2,128)S(1)}, f32[2,1024]{1,0:T(2,128)S(1)}, f32[2,1024,128]{2,1,0:T(8,128)S(1)}) %tuple.78, (s32[]{:T(128)}, s32[1024]{0:T(1024)S(1)}, s32[]{:T(128)}, ...), branch_computations={%region_5.5_spmd, %region_6.8_spmd} | conditional | flops 1115166720 | bytes 35348560 | solution.py:115
  245.0 4.2 %fusion.10 = f32[2,1024,128]{2,1,0:T(8,128)S(1)} fusion(bf16[1024,2,128]{0,2,1:T(8,128)(2,1)S(1)} %bitcast.65, f32[2,1024,1024]{2,1,0:T(8,128)S(1)} %get-tuple-element.336, f32[2,1024]{1,0:T(2,128)S(1)} %max.2, f32[2,1024]{1,0:T(2,128)S(1)} %dynamic-slice_bitcast_fusion, f32[2,1024]{1,0:T(2,128)S(1)} %get-tuple-element.230, ...), kind=kOutput, calls=%fused_computation.10 | convolution fusion | flops 552075264 | bytes 12091392 | tf_op jit(solution)/shard_map/while/body/eval_jaxpr/cond/branch_1_fun/hqk,khd->hqd/dot_general | solution.py:103
  249.7 7.1 %add_convert_fusion = bf16[1024,2048]{1,0:T(8,128)(2,1)} fusion(f32[1024,2048]{1,0:T(8,128)} %fusion.51, bf16[1024,256]{0,1:T(8,128)(2,1)S(1)} %bitcast.67, bf16[2048,2048]{1,0:T(8,128)(2,1)} %param.23, s32[]{:T(128)S(6)} %select_n.19), kind=kOutput, calls=%fused_computation.21 | convolution fusion | flops 1077936128 | bytes 14155780 | tf_op jit(solution)/shard_map/dot_general | solution.py:126
  256.8 56.6 %reduce-scatter.2.cloned.1.call-done = bf16[256,2048]{1,0:T(8,128)(2,1)} async-done(((bf16[1024,2048]{1,0:T(8,128)(2,1)}), bf16[256,2048]{1,0:T(8,128)(2,1)}) %reduce-scatter.2.cloned.1.call-update) | async-done | bytes 1048592 | tf_op jit(solution)/shard_map/reduce_scatter | solution.py:125
  (108 shorter events, 54.4 us)
Async XLA Ops:
  6.5 1.2 copy-start
  6.5 10.3 %copy-start.6 = (bf16[2048,256]{1,0:T(8,128)(2,1)S(1)}, bf16[2048,256]{1,0:T(8,128)(2,1)}, u32[]{:S(2)}) copy-start(bf16[2048,256]{1,0:T(8,128)(2,1)} %param.19) | copy-start | bytes 3145732
  6.5 78.8 %all-gather.3.cloned.1.call-start = ((), (), s32[]{:S(2)}) async-start(), calls=%async_computation.1 | async-start | bytes 4718592 | tf_op jit(solution)/shard_map/all_gather | solution.py:69
  12.0 8.4 %copy-start.7 = (bf16[2048,256]{1,0:T(8,128)(2,1)S(1)}, bf16[2048,256]{1,0:T(8,128)(2,1)}, u32[]{:S(2)}) copy-start(bf16[2048,256]{1,0:T(8,128)(2,1)} %param.18) | copy-start | bytes 3145732
  12.0 146.9 %all-gather.5.cloned.1.call-start = ((), (), s32[]{:S(2)}) async-start(), calls=%async_computation.2 | async-start | bytes 4718592 | tf_op jit(solution)/shard_map/all_gather | solution.py:70
  16.7 296.7 %reduce-scatter.2.cloned.1.call-start = ((), (), s32[]{:S(2)}) async-start(), calls=%async_computation.3 | async-start | bytes 5242880 | tf_op jit(solution)/shard_map/reduce_scatter | solution.py:125
  16.8 3.6 %copy-start.5 = (bf16[1024,2048]{1,0:T(8,128)(2,1)S(1)}, bf16[1024,2048]{1,0:T(8,128)(2,1)}, u32[]{:S(2)}) copy-start(bf16[1024,2048]{1,0:T(8,128)(2,1)} %param.14) | copy-start | bytes 12582916
  21.7 7.5 %copy-start.3 = (f32[31,256]{1,0:T(8,128)S(1)}, f32[31,256]{1,0:T(8,128)}, u32[]{:S(2)}) copy-start(f32[31,256]{1,0:T(8,128)} %param.20) | copy-start | bytes 95236
  21.7 7.6 %copy-start.2 = (f32[1024,2]{0,1:T(2,128)S(1)}, f32[1024,2]{0,1:T(2,128)}, u32[]{:S(2)}) copy-start(f32[1024,2]{0,1:T(2,128)} %param.22) | copy-start | bytes 24580
  21.7 36.3 %collective-permute-start = (bf16[30,256]{1,0:T(8,128)(2,1)S(1)}, bf16[30,256]{1,0:T(8,128)(2,1)S(1)}, u32[]{:S(2)}, u32[]{:S(2)}) collective-permute-start(bf16[30,256]{1,0:T(8,128)(2,1)S(1)} %slice.252), channel_id=1, source_target_pairs={{0,4},{4,8},{8,12},{12,16},{16,20},{20,24},{24,28},{1,5},{5,9},{9,... | collective-permute-start | bytes 46088 | tf_op jit(solution)/shard_map/ppermute | solution.py:17
  58.2 17.0 %copy-start.4 = (f32[256]{0:T(256)S(1)}, f32[256]{0:T(256)}, u32[]{:S(2)}) copy-start(f32[256]{0:T(256)} %param.21) | copy-start | bytes 3076
  249.7 63.7 %copy-start.1 = (bf16[2048,256]{1,0:T(8,128)(2,1)S(1)}, bf16[2048,256]{1,0:T(8,128)(2,1)}, u32[]{:S(2)}) copy-start(bf16[2048,256]{1,0:T(8,128)(2,1)} %param.16) | copy-start | bytes 3145732
Sparse Core Ops, SparseCore 0:
  12.1 73.1 all-gather.2
  87.5 71.3 all-gather.4
  256.9 56.4 reduce-scatter.1
where the time goes:
time: 322 us; the launch traced here: 320 us
  waiting for transfers between devices  128 us (40%)
  matrix products  78.5 us (24%)
  blocking collectives  41 us (13%)
  other arithmetic  30.7 us (10%)
  local copies, waits for them, and re-layouts  23.8 us (7%)
  between operations  13.3 us (4%)
  starting transfers between devices  3.47 us (1%)
    all_gather x1, waiting for transfers between devices, on_device(): piece_values = lax.all_gather(value_rows, 'sp', axis=0, tiled=True)  67.1 us
    reduce_scatter x1, waiting for transfers between devices, on_device(): lax.psum_scatter((projected + jnp.dot(attn_rows, attn_weight, preferred_e...  56.6 us
    dot_general x7, matrix products, attend(): jnp.einsum('hqk,khd->hqd', weights.astype(jnp.bfloat16), shard_values, pr...  29.6 us
    all_gather x1, blocking collectives, on_device(): gates_all = lax.all_gather(log_forget, 'sp', axis=0, tiled=True)  28.8 us
    reduce_sum x7, other arithmetic, attend(): new_sum = running_sum * rescale + jnp.sum(weights, axis=2)  21 us
    dot_general x7, matrix products, attend(): jnp.einsum('qhd,khd->hqk', query_heads, shard_keys, preferred_element_typ...  18.5 us
    unnamed x19, local copies, waits for them, and re-layouts  14.3 us
    dynamic_slice x7, local copies, waits for them, and re-layouts, attend(): lax.dynamic_slice_in_dim(piece_values, offset, block_rows, 0)  8.95 us
  transfers between devices with their start and end apart: 4, of which 3 were waited for; matrix products, arithmetic and copies ran while one was open for 10% of the time, Pallas kernels for 0%

commit v1 on v0

v1 whole, which is shorter than its diff:
```python
import functools

import jax
import jax.numpy as jnp
from jax import lax
from jax.experimental import pallas as pl
from jax.experimental.pallas import tpu as pltpu
from jax.sharding import PartitionSpec as P

HEAD_DIM = 128
NORM_EPS = 1e-05
LOG2E = 1.4426950408889634
GATE_PARTS = 3


def split_gates(gates):
    high = lax.reduce_precision(gates, 8, 7)
    middle = lax.reduce_precision(gates - high, 8, 7)
    low = gates - high - middle
    return jnp.stack([high, middle, low]).astype(jnp.bfloat16)


def flash_body(
    info_ref, q_ref, fq_ref, kv_ref, *refs, heads, rows, causal, first, last, gate_rows
):
    if first:
        outs = refs
    else:
        acc_in, max_in, sum_in = refs[:3]
        outs = refs[3:]
    width = heads * HEAD_DIM
    tile = q_ref.shape[0]
    q_first = info_ref[0] + lax.rem(pl.program_id(0) * tile, rows)
    q_first = jnp.where(pl.program_id(0) * tile >= rows, q_first + info_ref[1], q_first)
    key_first = info_ref[2]
    lanes = kv_ref.shape[1]

    def step(old):
        for h in range(heads):
            columns = slice(h * HEAD_DIM, (h + 1) * HEAD_DIM)
            keys = kv_ref[:rows, columns]
            values = kv_ref[:rows, width + h * HEAD_DIM : width + (h + 1) * HEAD_DIM]
            base = rows + h * GATE_PARTS * gate_rows
            packed = kv_ref[base : base + GATE_PARTS * gate_rows, :].astype(jnp.float32)
            pieces = []
            for g in range(gate_rows):
                total = packed[g : g + 1]
                for part in range(1, GATE_PARTS):
                    total = total + packed[part * gate_rows + g : part * gate_rows + g + 1]
                pieces.append(total)
            gates = jnp.concatenate(pieces, axis=1)
            bias = (fq_ref[h : h + 1, 0:1] - gates) * LOG2E
            scores = lax.dot_general(
                q_ref[:, columns],
                keys,
                (((1,), (1,)), ((), ())),
                preferred_element_type=jnp.float32,
            )
            scores = scores * (HEAD_DIM ** (-0.5) * LOG2E) + bias
            if causal:
                row_pos = q_first + lax.broadcasted_iota(jnp.int32, scores.shape, 0)
                key_pos = key_first + lax.broadcasted_iota(jnp.int32, scores.shape, 1)
                scores = jnp.where(key_pos <= row_pos, scores, -1e30)
            block_max = jnp.max(scores, axis=1, keepdims=True)
            if first:
                new_max = block_max
                weights = jnp.exp2(scores - new_max)
                new_sum = jnp.sum(weights, axis=1, keepdims=True)
            else:
                old_max = max_in[:, columns][:, :1]
                new_max = jnp.maximum(old_max, block_max)
                weights = jnp.exp2(scores - new_max)
                rescale = jnp.exp2(old_max - new_max)
                new_sum = sum_in[:, columns][:, :1] * rescale + jnp.sum(
                    weights, axis=1, keepdims=True
                )
            mixture = jnp.dot(
                weights.astype(jnp.bfloat16), values, preferred_element_type=jnp.float32
            )
            if not first:
                mixture = acc_in[:, columns] * rescale + mixture
            if last:
                outs[0][:, columns] = (mixture / new_sum).astype(jnp.bfloat16)
            else:
                outs[0][:, columns] = mixture
                outs[1][:, columns] = jnp.broadcast_to(new_max, (tile, HEAD_DIM))
                outs[2][:, columns] = jnp.broadcast_to(new_sum, (tile, HEAD_DIM))

    def keep():
        if last:
            for h in range(heads):
                columns = slice(h * HEAD_DIM, (h + 1) * HEAD_DIM)
                outs[0][:, columns] = (acc_in[:, columns] / sum_in[:, columns]).astype(
                    jnp.bfloat16
                )
        elif first:
            outs[0][...] = jnp.zeros_like(outs[0])
            outs[1][...] = jnp.full_like(outs[1], -1e30)
            outs[2][...] = jnp.zeros_like(outs[2])
        else:
            outs[0][...] = acc_in[...]
            outs[1][...] = max_in[...]
            outs[2][...] = sum_in[...]

    needed = info_ref[3] > 0
    if causal:
        needed = jnp.logical_and(needed, key_first <= q_first + (tile - 1))
    pl.when(needed)(lambda: step(None))
    pl.when(jnp.logical_not(needed))(keep)


def flash(info, q, fq, kv, state, *, heads, rows, tile, causal, last, gate_rows):
    total = q.shape[0]
    width = heads * HEAD_DIM
    row_spec = pl.BlockSpec((tile, width), lambda i: (i, 0))
    in_specs = [
        pl.BlockSpec(memory_space=pltpu.SMEM),
        row_spec,
        pl.BlockSpec((None,) + fq.shape[1:], lambda i: (i, 0, 0)),
        pl.BlockSpec(kv.shape, lambda i: (0, 0)),
    ]
    operands = [info, q, fq, kv]
    if state is not None:
        in_specs += [row_spec] * 3
        operands += list(state)
    if last:
        out_shape = jax.ShapeDtypeStruct((total, width), jnp.bfloat16)
        out_specs = row_spec
    else:
        out_shape = [jax.ShapeDtypeStruct((total, width), jnp.float32)] * 3
        out_specs = [row_spec] * 3
    return pl.pallas_call(
        functools.partial(
            flash_body,
            heads=heads,
            rows=rows,
            causal=causal,
            first=state is None,
            last=last,
            gate_rows=gate_rows,
        ),
        grid=(total // tile,),
        in_specs=in_specs,
        out_specs=out_specs,
        out_shape=out_shape,
        compiler_params=pltpu.CompilerParams(
            dimension_semantics=("arbitrary",), vmem_limit_bytes=40 * 1024 * 1024
        ),
        cost_estimate=pl.CostEstimate(
            flops=total * rows * width * 16,
            bytes_accessed=total * width * 24,
            transcendentals=total * rows * heads,
        ),
        name="flash",
    )(*operands)


def on_device(
    inputs,
    w_query,
    w_key,
    w_value,
    w_glu_value,
    w_glu_gate,
    conv_taps,
    conv_gain,
    log_forget,
    w_out,
):
    f32 = jnp.float32
    tok_rows = inputs.shape[0]
    channels = w_glu_value.shape[1]
    heads_here = w_query.shape[1] // HEAD_DIM
    tp_count = lax.axis_size("tp")
    sp_count = lax.axis_size("sp")
    sp_place = lax.axis_index("sp")
    total_channels = channels * tp_count
    out_rows = tok_rows // tp_count
    group = 2 if heads_here % 2 == 0 and sp_count % 2 == 0 else 1
    heads = heads_here // group
    width = heads * HEAD_DIM
    place = lax.rem(sp_place, group)
    block = sp_place // group
    blocks = sp_count // group
    gate_rows = tok_rows // (2 * width)
    pad_rows = -(heads * GATE_PARTS * gate_rows) % 16

    def swap(value):
        return lax.ppermute(value, "sp", [(i, i ^ 1) for i in range(sp_count)])

    def hop(value):
        return lax.ppermute(
            value, "sp", [(i, i + group) for i in range(sp_count - group)]
        )

    def columns_of(array, which, size):
        return lax.dynamic_slice_in_dim(array, which * size, size, 1)

    def keys_and_values(which):
        weight = jnp.concatenate(
            [columns_of(w_key, which, width), columns_of(w_value, which, width)], axis=1
        )
        both = jnp.dot(inputs, weight, preferred_element_type=f32).astype(jnp.bfloat16)
        gates = columns_of(log_forget, which, heads).T
        extra = jnp.swapaxes(split_gates(gates), 0, 1).reshape(-1, 2 * width)
        extra = jnp.pad(extra, ((0, pad_rows), (0, 0)))
        return jnp.concatenate([both, extra], axis=0), gates

    if group == 2:
        kv_send, _ = keys_and_values(1 - place)
        kv_partner = swap(kv_send)
        kv_own, gates_own = keys_and_values(place)
        halves = [kv_own, kv_partner]
    else:
        kv_own, gates_own = keys_and_values(place)
        halves = [kv_own]
    query_rows = jnp.dot(inputs, w_query, preferred_element_type=f32).astype(jnp.bfloat16)
    q = columns_of(query_rows, place, width)
    if group == 2:
        q_partner = swap(columns_of(query_rows, 1 - place, width))
        q = jnp.concatenate([q, q_partner], axis=0)

    glu_value = jnp.dot(inputs, w_glu_value, preferred_element_type=f32)
    glu_gate = jnp.dot(inputs, w_glu_gate, preferred_element_type=f32)
    gated = (glu_value * jax.nn.sigmoid(glu_gate)).astype(jnp.bfloat16)
    kernel = conv_taps.shape[0]
    halo = -(-(kernel - 1) // 16) * 16
    halo_rows = lax.ppermute(
        gated[tok_rows - halo :], "sp", [(i, i + 1) for i in range(sp_count - 1)]
    )
    padded = jnp.concatenate([halo_rows, gated], axis=0)
    windows = jnp.concatenate(
        [padded[t * out_rows : t * out_rows + out_rows + halo] for t in range(tp_count)], axis=0
    )
    windows = lax.all_to_all(windows, "tp", 0, 0, tiled=True).reshape(
        tp_count, out_rows + halo, channels
    )
    parameters = lax.all_gather(
        jnp.concatenate([conv_taps, conv_gain[None]], axis=0), "tp", axis=0
    )
    wide = windows.astype(f32)
    conv_sum = jnp.zeros((tp_count, out_rows, channels), f32)
    for offset in range(kernel):
        start = offset + halo - (kernel - 1)
        conv_sum = conv_sum + parameters[:, offset : offset + 1] * wide[:, start : start + out_rows]
    mean_value = jnp.sum(conv_sum, axis=(0, 2), keepdims=True) / total_channels
    centered = conv_sum - mean_value
    spread = jnp.sum(centered * centered, axis=(0, 2), keepdims=True) / total_channels
    conv_rows = jax.nn.silu(
        centered * lax.rsqrt(spread + NORM_EPS) * parameters[:, kernel : kernel + 1]
    ).astype(jnp.bfloat16)
    conv_rows = jnp.swapaxes(conv_rows, 0, 1).reshape(out_rows, total_channels)
    projected = jnp.dot(conv_rows, w_out[:total_channels], preferred_element_type=f32)

    tile = min(512, tok_rows)
    tiles_half = tok_rows // tile

    def packed_gates(half):
        extra = half[tok_rows : tok_rows + heads * GATE_PARTS * gate_rows].astype(f32)
        return extra.reshape(heads, GATE_PARTS, tok_rows).sum(axis=1)

    fq_parts = [gates_own] + [packed_gates(half) for half in halves[1:]]
    fq = jnp.concatenate(
        [part.reshape(heads, tiles_half, tile)[:, :, 0].T for part in fq_parts], axis=0
    )
    fq = jnp.broadcast_to(fq[:, :, None], fq.shape + (HEAD_DIM,))
    rows_own = place * tok_rows
    rows_partner = (group - 1 - place) * tok_rows
    offsets = [rows_own, rows_partner]

    def run(half, key_first, valid, state, causal, last):
        info = jnp.stack(
            [rows_own, rows_partner - rows_own, key_first, valid]
        ).astype(jnp.int32)
        return flash(
            info,
            q,
            fq,
            half,
            state,
            heads=heads,
            rows=tok_rows,
            tile=tile,
            causal=causal,
            last=last,
            gate_rows=gate_rows,
        )

    state = None
    for number in range(blocks):
        ready = halves
        if number < blocks - 1:
            halves = [hop(half) for half in ready]
        for part, half in enumerate(ready):
            finished = number == blocks - 1 and part == len(ready) - 1
            valid = (block >= number).astype(jnp.int32)
            state = run(half, offsets[part], valid, state, number == 0, finished)
    attn = state
    if group == 2:
        back = swap(attn[tok_rows:])
        mine = attn[:tok_rows]
        first_head = jnp.where(place == 0, mine, back)
        second_head = jnp.where(place == 0, back, mine)
        attn = jnp.concatenate([first_head, second_head], axis=1)
    attn = lax.all_to_all(attn, "tp", 0, 0, tiled=True)
    attn = jnp.swapaxes(attn.reshape(tp_count, out_rows, heads_here * HEAD_DIM), 0, 1)
    attn = attn.reshape(out_rows, tp_count * heads_here * HEAD_DIM)
    return (
        projected + jnp.dot(attn, w_out[total_channels:], preferred_element_type=f32)
    ).astype(jnp.bfloat16)


def solution(mesh):
    in_specs = (
        P("sp", None),
        P(None, "tp"),
        P(None, "tp"),
        P(None, "tp"),
        P(None, "tp"),
        P(None, "tp"),
        P(None, "tp"),
        P("tp"),
        P("sp", "tp"),
        P(),
    )
    out_specs = P(("sp", "tp"), None)
    return jax.shard_map(
        on_device, mesh=mesh, in_specs=in_specs, out_specs=out_specs, check_vma=False
    )
```

time: 322 us -> 177 us (0.55)
  waiting for transfers between devices: 128 us -> 26.7 us
  Pallas kernels: 0 us -> 59.7 us
  matrix products: 78.5 us -> 19.2 us
  blocking collectives: 41 us -> 5.42 us
  starting transfers between devices: 3.47 us -> 21.8 us
  between operations: 13.3 us -> 0.7 us
  other arithmetic: 30.7 us -> 22.4 us
  local copies, waits for them, and re-layouts: 23.8 us -> 19.9 us
    all_gather x2 -> x0, waiting for transfers between devices: 71.5 us -> none  [the longest x1 67.1 us: on_device(): piece_values = lax.all_gather(value_rows, 'sp', axis=0, tiled=True)]
    pallas_call x0 -> x8, Pallas kernels: none -> 59.7 us  [flash(): pl.pallas_call(functools.partial(flash_body, heads=heads, rows=rows, caus...]
    dot_general x21 -> x7, matrix products: 78.5 us -> 19.2 us  [the longest x2 4.81 us: keys_and_values(): jnp.dot(inputs, weight, preferred_element_type=f32).astype(jnp.bfloat16)]
    reduce_scatter x1 -> x0, waiting for transfers between devices: 56.6 us -> none  [on_device(): lax.psum_scatter((projected + jnp.dot(attn_rows, attn_weight, preferred_e...]
    all_gather x1, blocking collectives: 28.8 us -> 5.42 us  [on_device(): lax.all_gather(jnp.concatenate([conv_taps, conv_gain[None]], axis=0), 'tp...]
    all_to_all x0 -> x2, waiting for transfers between devices: none -> 16.1 us  [the longest x1 8.38 us: on_device(): attn = lax.all_to_all(attn, 'tp', 0, 0, tiled=True)]
    psum x2 -> x0, blocking collectives: 12.3 us -> none  [the longest x1 6.21 us: on_device(): lax.psum(jnp.sum(centered * centered, axis=1), 'tp') / total_channels]
    unnamed x19 -> x52, local copies, waits for them, and re-layouts: 14.3 us -> 2.13 us
  transfers between devices with their start and end apart: 4 -> 12, of which waited for: 3 -> 5; matrix products, arithmetic and copies ran while one was open for 10% -> 26% of each run, Pallas kernels for 0% -> 29%
where the time goes in v1:
time: 177 us; the launch traced here: 176 us
  Pallas kernels  59.7 us (34%)
  waiting for transfers between devices  26.7 us (15%)
  other arithmetic  22.4 us (13%)
  starting transfers between devices  21.8 us (12%)
  local copies, waits for them, and re-layouts  19.9 us (11%)
  matrix products  19.2 us (11%)
  blocking collectives  5.42 us (3%)
    pallas_call x8, Pallas kernels, flash(): pl.pallas_call(functools.partial(flash_body, heads=heads, rows=rows, caus...  59.7 us
    reduce_sum x1, other arithmetic, on_device(): mean_value = jnp.sum(conv_sum, axis=(0, 2), keepdims=True) / total_channels  15.1 us
    all_to_all x1, waiting for transfers between devices, on_device(): attn = lax.all_to_all(attn, 'tp', 0, 0, tiled=True)  8.38 us
    mul x15, local copies, waits for them, and re-layouts, on_device(): parameters[:, offset:offset + 1] * wide[:, start:start + out_rows]  8.32 us
    ppermute x6, starting transfers between devices, hop(): lax.ppermute(value, 'sp', [(i, i + group) for i in range(sp_count - group)])  7.91 us
    all_to_all x1, waiting for transfers between devices, on_device(): lax.all_to_all(windows, 'tp', 0, 0, tiled=True)  7.75 us
    ppermute x3, waiting for transfers between devices, swap(): return lax.ppermute(value, 'sp', [(i, i ^ 1) for i in range(sp_count)])  6.27 us
    all_gather x1, blocking collectives, on_device(): lax.all_gather(jnp.concatenate([conv_taps, conv_gain[None]], axis=0), 'tp...  5.42 us
  transfers between devices with their start and end apart: 12, of which 5 were waited for; matrix products, arithmetic and copies ran while one was open for 26% of the time, Pallas kernels for 29%

profile of v1, /device:TPU:24, one launch (start us, length us, event | category | flops | bytes accessed | tf_op | source)
XLA Modules:
  0.0 175.8 jit_solution(17592850868882969916)
XLA Ops:
  1.2 4.0 %fusion.12 = f32[1024,256]{1,0:T(8,128)S(1)} fusion(bf16[1024,2048]{1,0:T(8,128)(2,1)} %param.10, bf16[2048,256]{1,0:T(8,128)(2,1)S(1)} %copy-done), kind=kOutput, calls=%fused_computation.10 | convolution fusion | flops 1074528256 | bytes 6291456 | tf_op jit(solution)/shard_map/dot_general | solution.py:224
  7.2 3.4 %collective-permute-start = (bf16[32,256]{1,0:T(8,128)(2,1)}, bf16[32,256]{1,0:T(8,128)(2,1)S(1)}, u32[]{:S(2)}, u32[]{:S(2)}) collective-permute-start(bf16[32,256]{1,0:T(8,128)(2,1)} %slice.301), channel_id=1, source_target_pairs={{0,4},{4,8},{8,12},{12,16},{16,20},{20,24},{24,28},{1,5},{5,9},{9,... | collective-permute-start | bytes 49160 | tf_op jit(solution)/shard_map/ppermute | solution.py:228
  10.7 2.4 %constant_dynamic-slice_fusion = (bf16[2048,128]{1,0:T(8,128)(2,1)S(1)}, bf16[2048,128]{1,0:T(8,128)(2,1)S(1)}, bf16[2048,128]{1,0:T(8,128)(2,1)S(1)}, bf16[2048,128]{1,0:T(8,128)(2,1)}) fusion(bf16[2048,256]{1,0:T(8,128)(2,1)S(1)} %copy-done.2, s32[]{:T(128)S(6)} %select_n.35, s32[]{:T(128)S(6)} %select_n.36, bf16[2048,256]{1,0:T(8,128)(2,1)} %param.12), kind=kLoop, calls=%fused_computation.147 | loop fusion | bytes 4194312 | tf_op jit(solution)/shard_map/dynamic_slice | solution.py:197
  17.3 2.0 %collective-permute-start.1 = (bf16[1024,128]{1,0:T(8,128)(2,1)}, bf16[1024,128]{1,0:T(8,128)(2,1)}, u32[]{:S(2)}, u32[]{:S(2)}) collective-permute-start(bf16[1024,128]{1,0:T(8,128)(2,1)} %get-tuple-element.63), channel_id=1, source_target_pairs={{0,4},{4,0},{8,12},{12,8},{16,20},{20,16},{24,28},{28,24},{1,5},{5... | collective-permute-start | bytes 786440 | tf_op jit(solution)/shard_map/ppermute | solution.py:189
  19.4 3.6 %fusion.15 = bf16[1024,256]{1,0:T(8,128)(2,1)S(1)} fusion(bf16[1024,2048]{1,0:T(8,128)(2,1)} %param.10, bf16[2048,128]{1,0:T(8,128)(2,1)S(1)} %get-tuple-element.55, bf16[2048,128]{1,0:T(8,128)(2,1)} %get-tuple-element.109), kind=kOutput, calls=%fused_computation.16 | convolution fusion | flops 1076101120 | bytes 5767168 | tf_op jit(solution)/shard_map/dot_general | solution.py:203
  23.0 1.3 collective-permute-start.6
  24.3 5.4 %all-gather = f32[128,256]{1,0:T(8,128)S(1)} all-gather(f32[32,256]{1,0:T(8,128)S(1)} %pad_maximum_fusion.2), channel_id=2, replica_groups=mesh['sp'=8,'tp'=4] {'tp'}, dimensions={0}, use_global_device_ids=true | all-gather | bytes 163840 | tf_op jit(solution)/shard_map/all_gather | solution.py:238
  33.9 1.3 copy_bitcast_fusion.21
  36.5 1.3 copy_bitcast_fusion.25
  41.8 1.9 %fusion.58 = bf16[1152,256]{1,0:T(8,128)(2,1)} fusion(bf16[1024,256]{1,0:T(8,128)(2,1)S(1)} %fusion.13, bf16[32,256]{1,0:T(8,128)(2,1)S(1)} %collective-permute-done, bf16[288,256]{1,0:T(8,128)(2,1)} %get-tuple-element.60, bf16[288,256]{1,0:T(8,128)(2,1)} %get-tuple-element.61, bf16[288,256]{1,0:T(8,128)(2,1)} %get-tuple-element.59), kind=kLoop, calls=%fused_computation.94 | loop fusion | flops 3538944 | bytes 1572864 | tf_op jit(solution)/shard_map/concatenate | solution.py:232
  43.7 4.2 %all-to-all-start = ((bf16[4,288,256]{2,1,0:T(8,128)(2,1)}), bf16[4,288,256]{2,1,0:T(8,128)(2,1)}, u32[]{:S(2)}, u32[]{:S(2)}) async-start(bf16[4,288,256]{2,1,0:T(8,128)(2,1)} %bitcast.119), calls=%async_computation | async-start | bytes 1179648 | tf_op jit(solution)/shard_map/all_to_all | solution.py:235
  49.7 7.7 %all-to-all-done = bf16[4,288,256]{2,1,0:T(8,128)(2,1)} async-done(((bf16[4,288,256]{2,1,0:T(8,128)(2,1)}), bf16[4,288,256]{2,1,0:T(8,128)(2,1)}, u32[]{:S(2)}, u32[]{:S(2)}) %all-to-all-start) | async-done | bytes 589856 | tf_op jit(solution)/shard_map/all_to_all | solution.py:235
  57.4 2.2 %copy.86 = bf16[4,288,256]{1,2,0:T(8,128)(2,1)} copy(bf16[4,288,256]{2,1,0:T(8,128)(2,1)} %all-to-all-done) | data formatting | bytes 1179648 | tf_op jit(solution)/shard_map/all_to_all | solution.py:235
  61.0 15.1 %fusion.66 = (f32[256]{0:T(256)S(1)}, f32[4,256,256]{1,2,0:T(8,128)}) fusion(f32[4,288,256]{1,2,0:T(8,128)S(1)} %convert_element_type.54, f32[4,256]{1,0:T(4,128)S(1)} %get-tuple-element.112, f32[4,256]{1,0:T(4,128)S(1)} %get-tuple-element.113, f32[4,256]{1,0:T(4,128)S(1)} %get-tuple-element.114, f32[4,256]{1,0:T(4,128)S(1)} %get-tuple-element.115, ...), kind=kLoop, calls=%fused_computation.174 | loop fusion | flops 16252672 | bytes 33682432 | tf_op jit(solution)/shard_map/reduce_sum | solution.py:246
  76.3 1.3 collective-permute-start.3
  77.7 6.8 %flash.8 = (f32[2048,128]{1,0:T(8,128)S(1)}, f32[2048,128]{1,0:T(8,128)S(1)}, f32[2048,128]{1,0:T(8,128)S(1)}) custom-call(s32[4]{0:T(128)S(1)} %get-tuple-element.49.info_ref, bf16[2048,128]{1,0:T(8,128)(2,1)S(1)} %pad_maximum_fusion.q_ref, f32[4,1,128]{2,1,0:T(1,128)S(1)} %broadcast_in_dim.15.fq_ref, bf16[1040,256]{1,0:T(8,128)(2,1)S(1)} %fusion.60.kv_ref), custom_call_target="tpu_custom_call" | custom-call | flops 4294967296 | bytes 6291456 | tf_op jit(solution)/shard_map/flash/pallas_call | solution.py:132
  84.6 1.5 collective-permute-start.7
  86.1 4.6 %flash.9 = (f32[2048,128]{1,0:T(8,128)S(1)}, f32[2048,128]{1,0:T(8,128)S(1)}, f32[2048,128]{1,0:T(8,128)S(1)}) custom-call(s32[4]{0:T(128)S(1)} %get-tuple-element.51.info_ref, bf16[2048,128]{1,0:T(8,128)(2,1)S(1)} %pad_maximum_fusion.q_ref, f32[4,1,128]{2,1,0:T(1,128)S(1)} %broadcast_in_dim.15.fq_ref, bf16[1040,256]{1,0:T(8,128)(2,1)S(1)} %collective-permute-done.2.kv_ref, ...), custom_call_target="tpu_custom_call" | custom-call | flops 4294967296 | bytes 6291456 | tf_op jit(solution)/shard_map/flash/pallas_call | solution.py:132
  90.7 8.0 %flash.10 = (f32[2048,128]{1,0:T(8,128)S(1)}, f32[2048,128]{1,0:T(8,128)S(1)}, f32[2048,128]{1,0:T(8,128)S(1)}) custom-call(s32[4]{0:T(128)S(1)} %get-tuple-element.102.info_ref, bf16[2048,128]{1,0:T(8,128)(2,1)S(1)} %pad_maximum_fusion.q_ref, f32[4,1,128]{2,1,0:T(1,128)S(1)} %broadcast_in_dim.15.fq_ref, ...), custom_call_target="tpu_custom_call" | custom-call | flops 4294967296 | bytes 6291456 | tf_op jit(solution)/shard_map/flash/pallas_call | solution.py:132
  98.7 1.3 collective-permute-start.4
  100.0 4.0 %collective-permute-done.7.kv_ref = bf16[1040,256]{1,0:T(8,128)(2,1)S(1)} collective-permute-done((bf16[1040,256]{1,0:T(8,128)(2,1)S(1)}, bf16[1040,256]{1,0:T(8,128)(2,1)S(1)}, u32[]{:S(2)}, u32[]{:S(2)}) %collective-permute-start.7) | collective-permute-done | bytes 532512 | tf_op jit(solution)/shard_map/ppermute | solution.py:192
  105.3 8.0 %flash.11 = (f32[2048,128]{1,0:T(8,128)S(1)}, f32[2048,128]{1,0:T(8,128)S(1)}, f32[2048,128]{1,0:T(8,128)S(1)}) custom-call(s32[4]{0:T(128)S(1)} %get-tuple-element.105.info_ref, bf16[2048,128]{1,0:T(8,128)(2,1)S(1)} %pad_maximum_fusion.q_ref, f32[4,1,128]{2,1,0:T(1,128)S(1)} %broadcast_in_dim.15.fq_ref, ...), custom_call_target="tpu_custom_call" | custom-call | flops 4294967296 | bytes 6291456 | tf_op jit(solution)/shard_map/flash/pallas_call | solution.py:132
  113.4 8.0 %flash.12 = (f32[2048,128]{1,0:T(8,128)S(1)}, f32[2048,128]{1,0:T(8,128)S(1)}, f32[2048,128]{1,0:T(8,128)S(1)}) custom-call(s32[4]{0:T(128)S(1)} %get-tuple-element.103.info_ref, bf16[2048,128]{1,0:T(8,128)(2,1)S(1)} %pad_maximum_fusion.q_ref, f32[4,1,128]{2,1,0:T(1,128)S(1)} %broadcast_in_dim.15.fq_ref, ...), custom_call_target="tpu_custom_call" | custom-call | flops 4294967296 | bytes 6291456 | tf_op jit(solution)/shard_map/flash/pallas_call | solution.py:132
  121.4 1.3 collective-permute-start.5
  122.7 8.1 %flash.13 = (f32[2048,128]{1,0:T(8,128)S(1)}, f32[2048,128]{1,0:T(8,128)S(1)}, f32[2048,128]{1,0:T(8,128)S(1)}) custom-call(s32[4]{0:T(128)S(1)} %get-tuple-element.106.info_ref, bf16[2048,128]{1,0:T(8,128)(2,1)S(1)} %pad_maximum_fusion.q_ref, f32[4,1,128]{2,1,0:T(1,128)S(1)} %broadcast_in_dim.15.fq_ref, ...), custom_call_target="tpu_custom_call" | custom-call | flops 4294967296 | bytes 6291456 | tf_op jit(solution)/shard_map/flash/pallas_call | solution.py:132
  130.8 8.0 %flash.14 = (f32[2048,128]{1,0:T(8,128)S(1)}, f32[2048,128]{1,0:T(8,128)S(1)}, f32[2048,128]{1,0:T(8,128)S(1)}) custom-call(s32[4]{0:T(128)S(1)} %get-tuple-element.104.info_ref, bf16[2048,128]{1,0:T(8,128)(2,1)S(1)} %pad_maximum_fusion.q_ref, f32[4,1,128]{2,1,0:T(1,128)S(1)} %broadcast_in_dim.15.fq_ref, ...), custom_call_target="tpu_custom_call" | custom-call | flops 4294967296 | bytes 6291456 | tf_op jit(solution)/shard_map/flash/pallas_call | solution.py:132
  139.2 8.0 %flash.15 = bf16[2048,128]{1,0:T(8,128)(2,1)S(1)} custom-call(s32[4]{0:T(128)S(1)} %get-tuple-element.107.info_ref, bf16[2048,128]{1,0:T(8,128)(2,1)S(1)} %pad_maximum_fusion.q_ref, f32[4,1,128]{2,1,0:T(1,128)S(1)} %broadcast_in_dim.15.fq_ref, bf16[1040,256]{1,0:T(8,128)(2,1)S(1)} %collective-permute-done.5.kv_ref, ...), custom_call_target="tpu_custom_call" | custom-call | flops 4294967296 | bytes 6291456 | tf_op jit(solution)/shard_map/flash/pallas_call | solution.py:132
  148.2 6.3 %collective-permute-done.9 = bf16[1024,128]{1,0:T(8,128)(2,1)S(1)} collective-permute-done((bf16[1024,128]{1,0:T(8,128)(2,1)S(1)}, bf16[1024,128]{1,0:T(8,128)(2,1)S(1)}, u32[]{:S(2)}, u32[]{:S(2)}) %collective-permute-start.9) | collective-permute-done | bytes 262176 | tf_op jit(solution)/shard_map/ppermute | solution.py:189
  155.6 3.5 %all-to-all-start.1 = ((bf16[4,256,256]{1,2,0:T(8,128)(2,1)}), bf16[4,256,256]{1,2,0:T(8,128)(2,1)S(1)}, u32[]{:S(2)}, u32[]{:S(2)}) async-start(bf16[4,256,256]{1,2,0:T(8,128)(2,1)} %copy.120), calls=%async_computation.1 | async-start | bytes 1048576 | tf_op jit(solution)/shard_map/all_to_all | solution.py:305
  159.5 8.4 %all-to-all-done.1 = bf16[4,256,256]{1,2,0:T(8,128)(2,1)S(1)} async-done(((bf16[4,256,256]{1,2,0:T(8,128)(2,1)}), bf16[4,256,256]{1,2,0:T(8,128)(2,1)S(1)}, u32[]{:S(2)}, u32[]{:S(2)}) %all-to-all-start.1) | async-done | bytes 524320 | tf_op jit(solution)/shard_map/all_to_all | solution.py:305
  167.9 3.5 %fusion = f32[256,2048]{1,0:T(8,128)S(1)} fusion(bf16[256,1024]{0,1:T(8,128)(2,1)S(1)} %bitcast.123, bf16[2048,2048]{1,0:T(8,128)(2,1)} %param.19), kind=kOutput, calls=%fused_computation | convolution fusion | flops 1073741824 | bytes 6815744 | tf_op jit(solution)/shard_map/dot_general | solution.py:309
  171.3 4.4 %fusion.7 = bf16[256,2048]{1,0:T(8,128)(2,1)} fusion(f32[256,2048]{1,0:T(8,128)S(1)} %fusion, bf16[256,1024]{0,1:T(8,128)(2,1)S(1)} %bitcast.124, bf16[2048,2048]{1,0:T(8,128)(2,1)} %param.19), kind=kOutput, calls=%fused_computation.5 | convolution fusion | flops 1074790400 | bytes 7864320 | tf_op jit(solution)/shard_map/dot_general | solution.py:253
  (115 shorter events, 24.3 us)
Async XLA Ops:
  0.0 5.2 %copy-start.20 = (bf16[1024,2048]{1,0:T(8,128)(2,1)S(1)}, bf16[1024,2048]{1,0:T(8,128)(2,1)}, u32[]{:S(2)}) copy-start(bf16[1024,2048]{1,0:T(8,128)(2,1)} %param.10) | copy-start | bytes 12582916
  0.0 5.3 %copy-start.22 = (bf16[2048,256]{1,0:T(8,128)(2,1)S(1)}, bf16[2048,256]{1,0:T(8,128)(2,1)}, u32[]{:S(2)}) copy-start(bf16[2048,256]{1,0:T(8,128)(2,1)} %param.14) | copy-start | bytes 3145732
  5.3 5.3 %copy-start.4 = (f32[1024,2]{0,1:T(2,128)S(1)}, f32[1024,2]{0,1:T(2,128)}, u32[]{:S(2)}) copy-start(f32[1024,2]{0,1:T(2,128)} %param.18) | copy-start | bytes 24580
  5.3 5.4 %copy-start.2 = (bf16[2048,256]{1,0:T(8,128)(2,1)S(1)}, bf16[2048,256]{1,0:T(8,128)(2,1)}, u32[]{:S(2)}) copy-start(bf16[2048,256]{1,0:T(8,128)(2,1)} %param.13) | copy-start | bytes 3145732
  7.2 34.6 %collective-permute-start = (bf16[32,256]{1,0:T(8,128)(2,1)}, bf16[32,256]{1,0:T(8,128)(2,1)S(1)}, u32[]{:S(2)}, u32[]{:S(2)}) collective-permute-start(bf16[32,256]{1,0:T(8,128)(2,1)} %slice.301), channel_id=1, source_target_pairs={{0,4},{4,8},{8,12},{12,16},{16,20},{20,24},{24,28},{1,5},{5,9},{9,... | collective-permute-start | bytes 49160 | tf_op jit(solution)/shard_map/ppermute | solution.py:228
  15.3 60.8 %collective-permute-start.2 = (bf16[1040,256]{1,0:T(8,128)(2,1)}, bf16[1040,256]{1,0:T(8,128)(2,1)S(1)}, u32[]{:S(2)}, u32[]{:S(2)}) collective-permute-start(bf16[1040,256]{1,0:T(8,128)(2,1)} %fusion.59), channel_id=1, source_target_pairs={{0,4},{4,0},{8,12},{12,8},{16,20},{20,16},{24,28},{28,24},{1,5},{5... | collective-permute-start | bytes 1597448 | tf_op jit(solution)/shard_map/ppermute | solution.py:189
  17.3 31.2 %collective-permute-start.1 = (bf16[1024,128]{1,0:T(8,128)(2,1)}, bf16[1024,128]{1,0:T(8,128)(2,1)}, u32[]{:S(2)}, u32[]{:S(2)}) collective-permute-start(bf16[1024,128]{1,0:T(8,128)(2,1)} %get-tuple-element.63), channel_id=1, source_target_pairs={{0,4},{4,0},{8,12},{12,8},{16,20},{20,16},{24,28},{28,24},{1,5},{5... | collective-permute-start | bytes 786440 | tf_op jit(solution)/shard_map/ppermute | solution.py:189
  23.0 61.6 %collective-permute-start.6 = (bf16[1040,256]{1,0:T(8,128)(2,1)S(1)}, bf16[1040,256]{1,0:T(8,128)(2,1)S(1)}, u32[]{:S(2)}, u32[]{:S(2)}) collective-permute-start(bf16[1040,256]{1,0:T(8,128)(2,1)S(1)} %fusion.60.kv_ref), channel_id=1, source_target_pairs={{0,8},{4,12},{8,16},{12,20},{16,24},{20,28},{1,9},{5,13},{9,17},{1... | collective-permute-start | bytes 1597448 | tf_op jit(solution)/shard_map/ppermute | solution.py:192
  43.7 13.7 %all-to-all-start = ((bf16[4,288,256]{2,1,0:T(8,128)(2,1)}), bf16[4,288,256]{2,1,0:T(8,128)(2,1)}, u32[]{:S(2)}, u32[]{:S(2)}) async-start(bf16[4,288,256]{2,1,0:T(8,128)(2,1)} %bitcast.119), calls=%async_computation | async-start | bytes 1179648 | tf_op jit(solution)/shard_map/all_to_all | solution.py:235
  49.5 11.3 %copy-start.5 = (f32[4,256]{1,0:T(4,128)S(1)}, f32[4,256]{1,0:T(4,128)}, u32[]{:S(2)}) copy-start(f32[4,256]{1,0:T(4,128)} %get-tuple-element.128) | copy-start | bytes 12292
  49.6 11.3 %copy-start.6 = (f32[4,256]{1,0:T(4,128)S(1)}, f32[4,256]{1,0:T(4,128)}, u32[]{:S(2)}) copy-start(f32[4,256]{1,0:T(4,128)} %get-tuple-element.129) | copy-start | bytes 12292
  49.6 11.3 %copy-start.7 = (f32[4,256]{1,0:T(4,128)S(1)}, f32[4,256]{1,0:T(4,128)}, u32[]{:S(2)}) copy-start(f32[4,256]{1,0:T(4,128)} %get-tuple-element.130) | copy-start | bytes 12292
  49.6 11.3 %copy-start.8 = (f32[4,256]{1,0:T(4,128)S(1)}, f32[4,256]{1,0:T(4,128)}, u32[]{:S(2)}) copy-start(f32[4,256]{1,0:T(4,128)} %get-tuple-element.131) | copy-start | bytes 12292
  49.6 11.3 %copy-start.9 = (f32[4,256]{1,0:T(4,128)S(1)}, f32[4,256]{1,0:T(4,128)}, u32[]{:S(2)}) copy-start(f32[4,256]{1,0:T(4,128)} %get-tuple-element.132) | copy-start | bytes 12292
  49.6 11.3 %copy-start.10 = (f32[4,256]{1,0:T(4,128)S(1)}, f32[4,256]{1,0:T(4,128)}, u32[]{:S(2)}) copy-start(f32[4,256]{1,0:T(4,128)} %get-tuple-element.133) | copy-start | bytes 12292
  49.6 11.3 %copy-start.11 = (f32[4,256]{1,0:T(4,128)S(1)}, f32[4,256]{1,0:T(4,128)}, u32[]{:S(2)}) copy-start(f32[4,256]{1,0:T(4,128)} %get-tuple-element.134) | copy-start | bytes 12292
  49.6 11.3 %copy-start.12 = (f32[4,256]{1,0:T(4,128)S(1)}, f32[4,256]{1,0:T(4,128)}, u32[]{:S(2)}) copy-start(f32[4,256]{1,0:T(4,128)} %get-tuple-element.135) | copy-start | bytes 12292
  49.6 11.3 %copy-start.13 = (f32[4,256]{1,0:T(4,128)S(1)}, f32[4,256]{1,0:T(4,128)}, u32[]{:S(2)}) copy-start(f32[4,256]{1,0:T(4,128)} %get-tuple-element.136) | copy-start | bytes 12292
  49.6 11.3 %copy-start.14 = (f32[4,256]{1,0:T(4,128)S(1)}, f32[4,256]{1,0:T(4,128)}, u32[]{:S(2)}) copy-start(f32[4,256]{1,0:T(4,128)} %get-tuple-element.137) | copy-start | bytes 12292
  49.6 11.3 %copy-start.15 = (f32[4,256]{1,0:T(4,128)S(1)}, f32[4,256]{1,0:T(4,128)}, u32[]{:S(2)}) copy-start(f32[4,256]{1,0:T(4,128)} %get-tuple-element.138) | copy-start | bytes 12292
  49.7 11.3 %copy-start.16 = (f32[4,256]{1,0:T(4,128)S(1)}, f32[4,256]{1,0:T(4,128)}, u32[]{:S(2)}) copy-start(f32[4,256]{1,0:T(4,128)} %get-tuple-element.139) | copy-start | bytes 12292
  49.7 11.3 %copy-start.17 = (f32[4,256]{1,0:T(4,128)S(1)}, f32[4,256]{1,0:T(4,128)}, u32[]{:S(2)}) copy-start(f32[4,256]{1,0:T(4,128)} %get-tuple-element.140) | copy-start | bytes 12292
  49.7 11.3 %copy-start.18 = (f32[4,256]{1,0:T(4,128)S(1)}, f32[4,256]{1,0:T(4,128)}, u32[]{:S(2)}) copy-start(f32[4,256]{1,0:T(4,128)} %get-tuple-element.141) | copy-start | bytes 12292
  61.0 16.5 %copy-start.24 = (f32[2]{0:T(128)S(1)}, f32[2]{0:T(128)}, u32[]{:S(2)}) copy-start(f32[2]{0:T(128)} %slice_reduce_fusion.1) | copy-start | bytes 28
  76.3 22.4 %collective-permute-start.3 = (bf16[1040,256]{1,0:T(8,128)(2,1)S(1)}, bf16[1040,256]{1,0:T(8,128)(2,1)S(1)}, u32[]{:S(2)}, u32[]{:S(2)}) collective-permute-start(bf16[1040,256]{1,0:T(8,128)(2,1)S(1)} %collective-permute-done.2.kv_ref), channel_id=1, source_target_pairs={{0,8},{4,12},{8,16},{12,20},{16,24},{20,28},{1,9},{5,13},{9,17},{1... | collective-permute-start | bytes 1597448 | tf_op jit(solution)/shard_map/ppermute | solution.py:192
  84.6 19.4 %collective-permute-start.7 = (bf16[1040,256]{1,0:T(8,128)(2,1)S(1)}, bf16[1040,256]{1,0:T(8,128)(2,1)S(1)}, u32[]{:S(2)}, u32[]{:S(2)}) collective-permute-start(bf16[1040,256]{1,0:T(8,128)(2,1)S(1)} %collective-permute-done.6.kv_ref), channel_id=1, source_target_pairs={{0,8},{4,12},{8,16},{12,20},{16,24},{20,28},{1,9},{5,13},{9,17},{1... | collective-permute-start | bytes 1597448 | tf_op jit(solution)/shard_map/ppermute | solution.py:192
  98.7 22.7 %collective-permute-start.4 = (bf16[1040,256]{1,0:T(8,128)(2,1)S(1)}, bf16[1040,256]{1,0:T(8,128)(2,1)S(1)}, u32[]{:S(2)}, u32[]{:S(2)}) collective-permute-start(bf16[1040,256]{1,0:T(8,128)(2,1)S(1)} %collective-permute-done.3.kv_ref), channel_id=1, source_target_pairs={{0,8},{4,12},{8,16},{12,20},{16,24},{20,28},{1,9},{5,13},{9,17},{1... | collective-permute-start | bytes 1597448 | tf_op jit(solution)/shard_map/ppermute | solution.py:192
  104.0 26.8 %collective-permute-start.8 = (bf16[1040,256]{1,0:T(8,128)(2,1)S(1)}, bf16[1040,256]{1,0:T(8,128)(2,1)S(1)}, u32[]{:S(2)}, u32[]{:S(2)}) collective-permute-start(bf16[1040,256]{1,0:T(8,128)(2,1)S(1)} %collective-permute-done.7.kv_ref), channel_id=1, source_target_pairs={{0,8},{4,12},{8,16},{12,20},{16,24},{20,28},{1,9},{5,13},{9,17},{1... | collective-permute-start | bytes 1597448 | tf_op jit(solution)/shard_map/ppermute | solution.py:192
  121.4 17.7 %collective-permute-start.5 = (bf16[1040,256]{1,0:T(8,128)(2,1)S(1)}, bf16[1040,256]{1,0:T(8,128)(2,1)S(1)}, u32[]{:S(2)}, u32[]{:S(2)}) collective-permute-start(bf16[1040,256]{1,0:T(8,128)(2,1)S(1)} %collective-permute-done.4.kv_ref), channel_id=1, source_target_pairs={{0,8},{4,12},{8,16},{12,20},{16,24},{20,28},{1,9},{5,13},{9,17},{1... | collective-permute-start | bytes 1597448 | tf_op jit(solution)/shard_map/ppermute | solution.py:192
  139.2 8.9 %copy-start.1 = (f32[4,256,256]{1,2,0:T(8,128)S(1)}, f32[4,256,256]{1,2,0:T(8,128)}, u32[]{:S(2)}) copy-start(f32[4,256,256]{1,2,0:T(8,128)} %get-tuple-element.48) | copy-start | bytes 3145732
  147.2 7.2 %collective-permute-start.9 = (bf16[1024,128]{1,0:T(8,128)(2,1)S(1)}, bf16[1024,128]{1,0:T(8,128)(2,1)S(1)}, u32[]{:S(2)}, u32[]{:S(2)}) collective-permute-start(bf16[1024,128]{1,0:T(8,128)(2,1)S(1)} %slice.371), channel_id=1, source_target_pairs={{0,4},{4,0},{8,12},{12,8},{16,20},{20,16},{24,28},{28,24},{1,5},{5... | collective-permute-start | bytes 786440 | tf_op jit(solution)/shard_map/ppermute | solution.py:189
  155.6 12.3 %all-to-all-start.1 = ((bf16[4,256,256]{1,2,0:T(8,128)(2,1)}), bf16[4,256,256]{1,2,0:T(8,128)(2,1)S(1)}, u32[]{:S(2)}, u32[]{:S(2)}) async-start(bf16[4,256,256]{1,2,0:T(8,128)(2,1)} %copy.120), calls=%async_computation.1 | async-start | bytes 1048576 | tf_op jit(solution)/shard_map/all_to_all | solution.py:305
  (5 other events, 15.7 us)

commit v2 on v1

v2 whole, which is shorter than its diff:
```python
import functools

import jax
import jax.numpy as jnp
from jax import lax
from jax.experimental import pallas as pl
from jax.experimental.pallas import tpu as pltpu
from jax.sharding import PartitionSpec as P

HEAD_DIM = 128
NORM_EPS = 1e-05
LOG2E = 1.4426950408889634
GATE_PARTS = 3
SUB_ROWS = 256


def split_gates(gates):
    high = lax.reduce_precision(gates, 8, 7)
    middle = lax.reduce_precision(gates - high, 8, 7)
    low = gates - high - middle
    return jnp.stack([high, middle, low]).astype(jnp.bfloat16)


def flash_body(
    info_ref,
    shift_ref,
    q_ref,
    kv_ref,
    *refs,
    heads,
    rows,
    sub,
    causal,
    first,
    last,
    gate_rows,
):
    if first:
        outs = refs
    else:
        acc_in, max_in, sum_in = refs[:3]
        outs = refs[3:]
    width = heads * HEAD_DIM
    tile = q_ref.shape[0]
    q_first = pl.program_id(0) * tile
    key_first = info_ref[0]

    def step():
        for h in range(heads):
            columns = slice(h * HEAD_DIM, (h + 1) * HEAD_DIM)
            keys = kv_ref[:rows, columns]
            values = kv_ref[:rows, width + h * HEAD_DIM : width + (h + 1) * HEAD_DIM]
            values = jnp.concatenate([values, jnp.ones_like(values)], axis=1)
            base = rows + h * GATE_PARTS * gate_rows
            packed = kv_ref[base : base + GATE_PARTS * gate_rows, :].astype(jnp.float32)
            pieces = []
            for g in range(gate_rows):
                total = packed[g : g + 1]
                for part in range(1, GATE_PARTS):
                    total = total + packed[part * gate_rows + g : part * gate_rows + g + 1]
                pieces.append(total)
            gates = jnp.concatenate(pieces, axis=1)
            bias = (shift_ref[h] - gates) * LOG2E
            for begin in range(0, tile, sub):
                here = slice(begin, begin + sub)
                scores = lax.dot_general(
                    q_ref[here, columns],
                    keys,
                    (((1,), (1,)), ((), ())),
                    preferred_element_type=jnp.float32,
                )
                scores = scores * (HEAD_DIM ** (-0.5) * LOG2E) + bias
                if causal:
                    ahead = q_first + begin - key_first
                    row_pos = ahead + lax.broadcasted_iota(jnp.int32, scores.shape, 0)
                    key_pos = lax.broadcasted_iota(jnp.int32, scores.shape, 1)
                    scores = jnp.where(key_pos <= row_pos, scores, -1e30)
                new_max = jnp.max(scores, axis=1, keepdims=True)
                if not first:
                    old_max = max_in[here, columns][:, :1]
                    new_max = jnp.maximum(old_max, new_max)
                weights = jnp.exp2(scores - new_max).astype(jnp.bfloat16)
                both = jnp.dot(weights, values, preferred_element_type=jnp.float32)
                mixture, new_sum = both[:, :HEAD_DIM], both[:, HEAD_DIM:]
                if not first:
                    rescale = jnp.exp2(old_max - new_max)
                    mixture = acc_in[here, columns] * rescale + mixture
                    new_sum = sum_in[here, columns] * rescale + new_sum
                if last:
                    outs[0][here, columns] = (mixture / new_sum).astype(jnp.bfloat16)
                else:
                    outs[0][here, columns] = mixture
                    outs[1][here, columns] = jnp.broadcast_to(new_max, mixture.shape)
                    outs[2][here, columns] = new_sum

    def keep():
        if last:
            outs[0][...] = (acc_in[...] / sum_in[...]).astype(jnp.bfloat16)
        elif first:
            outs[0][...] = jnp.zeros_like(outs[0])
            outs[1][...] = jnp.full_like(outs[1], -1e30)
            outs[2][...] = jnp.zeros_like(outs[2])
        else:
            outs[0][...] = acc_in[...]
            outs[1][...] = max_in[...]
            outs[2][...] = sum_in[...]

    needed = info_ref[1] > 0
    if causal:
        needed = jnp.logical_and(needed, key_first <= q_first + (tile - 1))
    pl.when(needed)(step)
    pl.when(jnp.logical_not(needed))(keep)


def flash(info, shift, q, kv, state, *, heads, rows, tile, sub, causal, last, gate_rows):
    total = q.shape[0]
    width = heads * HEAD_DIM
    row_spec = pl.BlockSpec((tile, width), lambda i: (i, 0))
    in_specs = [
        pl.BlockSpec(memory_space=pltpu.SMEM),
        pl.BlockSpec(memory_space=pltpu.SMEM),
        row_spec,
        pl.BlockSpec(kv.shape, lambda i: (0, 0)),
    ]
    operands = [info, shift, q, kv]
    if state is not None:
        in_specs += [row_spec] * 3
        operands += list(state)
    if last:
        out_shape = jax.ShapeDtypeStruct((total, width), jnp.bfloat16)
        out_specs = row_spec
    else:
        out_shape = [jax.ShapeDtypeStruct((total, width), jnp.float32)] * 3
        out_specs = [row_spec] * 3
    return pl.pallas_call(
        functools.partial(
            flash_body,
            heads=heads,
            rows=rows,
            sub=sub,
            causal=causal,
            first=state is None,
            last=last,
            gate_rows=gate_rows,
        ),
        grid=(total // tile,),
        in_specs=in_specs,
        out_specs=out_specs,
        out_shape=out_shape,
        compiler_params=pltpu.CompilerParams(
            dimension_semantics=("arbitrary",), vmem_limit_bytes=40 * 1024 * 1024
        ),
        cost_estimate=pl.CostEstimate(
            flops=total * rows * width * 16,
            bytes_accessed=total * width * 24,
            transcendentals=total * rows * heads,
        ),
        name="flash",
    )(*operands)


def conv_body(window_ref, out_ref, sums_ref, *, taps, halo, rows, total_channels):
    groups, _, channels = window_ref.shape
    table = rows + halo
    total = jnp.zeros((rows, 1), jnp.float32)
    for g in range(groups):
        parts = window_ref[g, table:, :].astype(jnp.float32)
        count = parts.shape[0] // GATE_PARTS
        weights = parts[:count] + parts[count : 2 * count] + parts[2 * count :]
        sums_ref[g, 0, :table, :] = window_ref[g, :table, :].astype(jnp.float32)
        sums_ref[g, 1, :count, :] = weights
    for g in range(groups):
        for c in range(0, channels, HEAD_DIM):
            lanes = slice(c, c + HEAD_DIM)
            acc = jnp.zeros((rows, HEAD_DIM), jnp.float32)
            for offset in range(taps):
                start = offset + halo - (taps - 1)
                acc = acc + sums_ref[g, 1, offset : offset + 1, lanes] * (
                    sums_ref[g, 0, start : start + rows, lanes]
                )
            total = total + jnp.sum(acc, axis=1, keepdims=True)
            sums_ref[g, 2, :rows, lanes] = acc
    mean_value = total / total_channels
    squares = jnp.zeros((rows, 1), jnp.float32)
    for g in range(groups):
        centered = sums_ref[g, 2, :rows, :] - mean_value
        squares = squares + jnp.sum(centered * centered, axis=1, keepdims=True)
    factor = lax.rsqrt(squares / total_channels + NORM_EPS)
    for g in range(groups):
        centered = sums_ref[g, 2, :rows, :] - mean_value
        values = centered * factor * sums_ref[g, 1, taps : taps + 1, :]
        out_ref[:, g * channels : (g + 1) * channels] = (
            values / (1.0 + jnp.exp(-values))
        ).astype(jnp.bfloat16)


def convolve(windows, *, taps, halo, rows, total_channels):
    groups, depth, channels = windows.shape
    return pl.pallas_call(
        functools.partial(
            conv_body, taps=taps, halo=halo, rows=rows, total_channels=total_channels
        ),
        out_shape=jax.ShapeDtypeStruct((rows, total_channels), jnp.bfloat16),
        scratch_shapes=[pltpu.VMEM((groups, 3, rows + halo, channels), jnp.float32)],
        compiler_params=pltpu.CompilerParams(vmem_limit_bytes=40 * 1024 * 1024),
        cost_estimate=pl.CostEstimate(
            flops=total_channels * rows * taps * 64, bytes_accessed=1 << 21, transcendentals=0
        ),
        name="convolve",
    )(windows)


def on_device(
    inputs,
    w_query,
    w_key,
    w_value,
    w_glu_value,
    w_glu_gate,
    conv_taps,
    conv_gain,
    log_forget,
    w_out,
):
    f32 = jnp.float32
    tok_rows = inputs.shape[0]
    channels = w_glu_value.shape[1]
    heads_here = w_query.shape[1] // HEAD_DIM
    tp_count = lax.axis_size("tp")
    sp_count = lax.axis_size("sp")
    sp_place = lax.axis_index("sp")
    total_channels = channels * tp_count
    out_rows = tok_rows // tp_count
    group = 2 if heads_here % 2 == 0 and sp_count % 2 == 0 else 1
    heads = heads_here // group
    width = heads * HEAD_DIM
    place = lax.rem(sp_place, group)
    block = sp_place // group
    blocks = sp_count // group
    gate_rows = tok_rows // (2 * width)
    pad_rows = -(heads * GATE_PARTS * gate_rows) % 16

    def swap(value):
        return lax.ppermute(value, "sp", [(i, i ^ 1) for i in range(sp_count)])

    def hop(value):
        return lax.ppermute(
            value, "sp", [(i, i + group) for i in range(sp_count - group)]
        )

    def columns_of(array, which, size):
        return lax.dynamic_slice_in_dim(array, which * size, size, 1)

    def keys_and_values(which):
        weight = jnp.concatenate(
            [columns_of(w_key, which, width), columns_of(w_value, which, width)], axis=1
        )
        both = jnp.dot(inputs, weight, preferred_element_type=f32).astype(jnp.bfloat16)
        gates = columns_of(log_forget, which, heads).T
        extra = jnp.swapaxes(split_gates(gates), 0, 1).reshape(-1, 2 * width)
        extra = jnp.pad(extra, ((0, pad_rows), (0, 0)))
        return jnp.concatenate([both, extra], axis=0), gates

    if group == 2:
        kv_send, _ = keys_and_values(1 - place)
        kv_partner = swap(kv_send)
        kv_own, gates_own = keys_and_values(place)
        halves = [kv_own, kv_partner]
    else:
        kv_own, gates_own = keys_and_values(place)
        halves = [kv_own]
    query_rows = jnp.dot(inputs, w_query, preferred_element_type=f32).astype(jnp.bfloat16)
    q = columns_of(query_rows, place, width)
    if group == 2:
        q_partner = swap(columns_of(query_rows, 1 - place, width))
        q = jnp.where(
            place == 0,
            jnp.concatenate([q, q_partner], axis=0),
            jnp.concatenate([q_partner, q], axis=0),
        )

    glu_value = jnp.dot(inputs, w_glu_value, preferred_element_type=f32)
    glu_gate = jnp.dot(inputs, w_glu_gate, preferred_element_type=f32)
    gated = (glu_value * jax.nn.sigmoid(glu_gate)).astype(jnp.bfloat16)
    kernel = conv_taps.shape[0]
    halo = -(-(kernel - 1) // 16) * 16
    halo_rows = lax.ppermute(
        gated[tok_rows - halo :], "sp", [(i, i + 1) for i in range(sp_count - 1)]
    )
    padded = jnp.concatenate([halo_rows, gated], axis=0)
    table = split_gates(jnp.concatenate([conv_taps, conv_gain[None]], axis=0))
    table = table.reshape(-1, channels)
    pieces = []
    for t in range(tp_count):
        pieces += [padded[t * out_rows : t * out_rows + out_rows + halo], table]
    windows = lax.all_to_all(jnp.concatenate(pieces, axis=0), "tp", 0, 0, tiled=True)
    windows = windows.reshape(tp_count, -1, channels)

    tile = min(512, tok_rows)
    shift = gates_own[:, 0]
    offsets = [place * tok_rows, (group - 1 - place) * tok_rows]

    def run(half, key_first, valid, state, causal, last):
        info = jnp.stack([key_first, valid]).astype(jnp.int32)
        return flash(
            info,
            shift,
            q,
            half,
            state,
            heads=heads,
            rows=tok_rows,
            tile=tile,
            sub=min(SUB_ROWS, tile),
            causal=causal,
            last=last,
            gate_rows=gate_rows,
        )

    state = None
    for number in range(blocks):
        ready = halves
        if number < blocks - 1:
            halves = [hop(half) for half in ready]
        for part, half in enumerate(ready):
            finished = number == blocks - 1 and part == len(ready) - 1
            valid = (block >= number).astype(jnp.int32)
            state = run(half, offsets[part], valid, state, number == 0, finished)
    windows, attn = lax.optimization_barrier((windows, state))
    if group == 2:
        members = [
            [
                (base + r) * tp_count + t
                for r in range(group)
                for t in range(tp_count)
            ]
            for base in range(0, sp_count, group)
        ]
        attn = lax.all_to_all(
            attn, ("sp", "tp"), 0, 0, axis_index_groups=members, tiled=True
        )
        attn = attn.reshape(group, tp_count, out_rows, width)
    else:
        attn = lax.all_to_all(attn, "tp", 0, 0, tiled=True)
        attn = attn.reshape(1, tp_count, out_rows, width)
    conv_rows = convolve(
        windows, taps=kernel, halo=halo, rows=out_rows, total_channels=total_channels
    )
    projected = jnp.dot(conv_rows, w_out[:total_channels], preferred_element_type=f32)
    attn = jnp.transpose(attn, (2, 1, 0, 3)).reshape(out_rows, -1)
    return (
        projected + jnp.dot(attn, w_out[total_channels:], preferred_element_type=f32)
    ).astype(jnp.bfloat16)


def solution(mesh):
    in_specs = (
        P("sp", None),
        P(None, "tp"),
        P(None, "tp"),
        P(None, "tp"),
        P(None, "tp"),
        P(None, "tp"),
        P(None, "tp"),
        P("tp"),
        P("sp", "tp"),
        P(),
    )
    out_specs = P(("sp", "tp"), None)
    return jax.shard_map(
        on_device, mesh=mesh, in_specs=in_specs, out_specs=out_specs, check_vma=False
    )
```

time: 177 us -> 135 us (0.76)
  other arithmetic: 22.4 us -> 2.91 us
  local copies, waits for them, and re-layouts: 19.9 us -> 6.42 us
  blocking collectives: 5.42 us -> 0 us
  Pallas kernels: 59.7 us -> 56.4 us
  waiting for transfers between devices: 26.7 us -> 28.8 us
    reduce_sum x3 -> x0, other arithmetic: 15.3 us -> none  [the longest x1 15.1 us: on_device(): mean_value = jnp.sum(conv_sum, axis=(0, 2), keepdims=True) / total_channels]
    ppermute x6, waiting for transfers between devices: 4.33 us -> 18 us  [hop(): lax.ppermute(value, 'sp', [(i, i + group) for i in range(sp_count - group)])]
    all_to_all x2, waiting for transfers between devices: 16.1 us -> 2.87 us  [the longest x1 2.87 us: on_device(): lax.all_to_all(attn, ('sp', 'tp'), 0, 0, axis_index_groups=members, tiled...]
    mul x15 -> x0, local copies, waits for them, and re-layouts: 8.32 us -> none  [on_device(): parameters[:, offset:offset + 1] * wide[:, start:start + out_rows]]
    ppermute x1, waiting for transfers between devices: 0.01 us -> 7.92 us  [on_device(): lax.ppermute(gated[tok_rows - halo:], 'sp', [(i, i + 1) for i in range(sp...]
    ppermute x3 -> x2, waiting for transfers between devices: 6.27 us -> 0.01 us  [swap(): return lax.ppermute(value, 'sp', [(i, i ^ 1) for i in range(sp_count)])]
    all_gather x1 -> x0, blocking collectives: 5.42 us -> none  [on_device(): lax.all_gather(jnp.concatenate([conv_taps, conv_gain[None]], axis=0), 'tp...]
    pallas_call x8 -> x9, Pallas kernels: 59.7 us -> 56.4 us  [the longest x8 50.8 us: flash(): pl.pallas_call(functools.partial(flash_body, heads=heads, rows=rows, sub=...]
  transfers between devices with their start and end apart: 12 -> 11, of which waited for: 5 -> 6; matrix products, arithmetic and copies ran while one was open for 26% -> 9% of each run, Pallas kernels for 29% -> 42%
where the time goes in v2:
time: 135 us
  Pallas kernels  56.4 us (42%)
  waiting for transfers between devices  28.8 us (21%)
  starting transfers between devices  20.7 us (15%)
  matrix products  18.9 us (14%)
  local copies, waits for them, and re-layouts  6.42 us (5%)
  other arithmetic  2.91 us (2%)
    pallas_call x8, Pallas kernels, flash(): pl.pallas_call(functools.partial(flash_body, heads=heads, rows=rows, sub=...  50.8 us
    ppermute x6, waiting for transfers between devices, hop(): lax.ppermute(value, 'sp', [(i, i + group) for i in range(sp_count - group)])  18 us
    ppermute x6, starting transfers between devices, hop(): lax.ppermute(value, 'sp', [(i, i + group) for i in range(sp_count - group)])  8.04 us
    ppermute x1, waiting for transfers between devices, on_device(): lax.ppermute(gated[tok_rows - halo:], 'sp', [(i, i + 1) for i in range(sp...  7.92 us
    pallas_call x1, Pallas kernels, convolve(): pl.pallas_call(functools.partial(conv_body, taps=taps, halo=halo, rows=ro...  5.69 us
    dot_general x2, matrix products, keys_and_values(): jnp.dot(inputs, weight, preferred_element_type=f32).astype(jnp.bfloat16)  4.84 us
    dot_general x1, matrix products, on_device(): jnp.dot(conv_rows, w_out[:total_channels], preferred_element_type=f32)  4.47 us
    all_to_all x1, starting transfers between devices, on_device(): lax.all_to_all(attn, ('sp', 'tp'), 0, 0, axis_index_groups=members, tiled...  3.71 us
  transfers between devices with their start and end apart: 11, of which 6 were waited for; matrix products, arithmetic and copies ran while one was open for 9% of the time, Pallas kernels for 42%

profile of v2, /device:TPU:24, one launch (start us, length us, event | category | flops | bytes accessed | tf_op | source)
XLA Modules:
  0.0 134.5 jit_solution(10289289515165889983)
XLA Ops:
  1.2 3.6 %convolution_convert_fusion.2 = bf16[1024,256]{1,0:T(8,128)(2,1)S(1)} fusion(bf16[1024,2048]{1,0:T(8,128)(2,1)} %param.10, bf16[2048,256]{1,0:T(8,128)(2,1)S(1)} %copy-done), kind=kOutput, calls=%fused_computation.14 | convolution fusion | flops 1074003968 | bytes 5767168 | tf_op jit(solution)/shard_map/dot_general | solution.py:272
  5.7 1.5 %collective-permute-start.1 = (bf16[1024,128]{1,0:T(8,128)(2,1)}, bf16[1024,128]{1,0:T(8,128)(2,1)}, u32[]{:S(2)}, u32[]{:S(2)}) collective-permute-start(bf16[1024,128]{1,0:T(8,128)(2,1)} %get-tuple-element.56), channel_id=1, source_target_pairs={{0,4},{4,0},{8,12},{12,8},{16,20},{20,16},{24,28},{28,24},{1,5},{5... | collective-permute-start | bytes 786440 | tf_op jit(solution)/shard_map/ppermute | solution.py:244
  7.3 1.3 constant_dynamic-slice_fusion
  12.5 3.6 %fusion.15 = bf16[1024,256]{1,0:T(8,128)(2,1)S(1)} fusion(bf16[1024,2048]{1,0:T(8,128)(2,1)} %param.10, bf16[2048,128]{1,0:T(8,128)(2,1)S(1)} %copy-done.4, bf16[2048,128]{1,0:T(8,128)(2,1)S(1)} %copy-done.5), kind=kOutput, calls=%fused_computation.16 | convolution fusion | flops 1076101120 | bytes 5767168 | tf_op jit(solution)/shard_map/dot_general | solution.py:258
  16.2 1.4 %collective-permute-start.6 = (bf16[1040,256]{1,0:T(8,128)(2,1)S(1)}, bf16[1040,256]{1,0:T(8,128)(2,1)S(1)}, u32[]{:S(2)}, u32[]{:S(2)}) collective-permute-start(bf16[1040,256]{1,0:T(8,128)(2,1)S(1)} %fusion.25.kv_ref), channel_id=1, source_target_pairs={{0,8},{4,12},{8,16},{12,20},{16,24},{20,28},{1,9},{5,13},{9,17},{1... | collective-permute-start | bytes 1597448 | tf_op jit(solution)/shard_map/ppermute | solution.py:247
  17.6 1.3 fusion.12
  19.0 1.2 fusion.13
  20.2 3.4 %collective-permute-start = (bf16[32,256]{1,0:T(8,128)(2,1)S(1)}, bf16[32,256]{1,0:T(8,128)(2,1)S(1)}, u32[]{:S(2)}, u32[]{:S(2)}) collective-permute-start(bf16[32,256]{1,0:T(8,128)(2,1)S(1)} %slice.32), channel_id=1, source_target_pairs={{0,4},{4,8},{8,12},{12,16},{16,20},{20,24},{24,28},{1,5},{5,9},{9,... | collective-permute-start | bytes 49160 | tf_op jit(solution)/shard_map/ppermute | solution.py:287
  24.9 7.9 %collective-permute-done = bf16[32,256]{1,0:T(8,128)(2,1)S(1)} collective-permute-done((bf16[32,256]{1,0:T(8,128)(2,1)S(1)}, bf16[32,256]{1,0:T(8,128)(2,1)S(1)}, u32[]{:S(2)}, u32[]{:S(2)}) %collective-permute-start) | collective-permute-done | bytes 16416 | tf_op jit(solution)/shard_map/ppermute | solution.py:287
  33.8 3.5 %all-to-all-start = ((bf16[4,384,256]{2,1,0:T(8,128)(2,1)}), bf16[4,384,256]{2,1,0:T(8,128)(2,1)S(1)}, u32[]{:S(2)}, u32[]{:S(2)}) async-start(bf16[4,384,256]{2,1,0:T(8,128)(2,1)} %bitcast.55), calls=%async_computation | async-start | bytes 1572864 | tf_op jit(solution)/shard_map/all_to_all | solution.py:296
  37.3 1.3 maximum_select_fusion.q_ref
  38.6 6.3 %flash.8 = (f32[2048,128]{1,0:T(8,128)S(1)}, f32[2048,128]{1,0:T(8,128)S(1)}, f32[2048,128]{1,0:T(8,128)S(1)}) custom-call(s32[2]{0:T(128)S(1)} %pad_add_fusion.6.info_ref, f32[1]{0:T(128)} %bitcast.7.shift_ref, bf16[2048,128]{1,0:T(8,128)(2,1)S(1)} %maximum_select_fusion.q_ref, bf16[1040,256]{1,0:T(8,128)(2,1)S(1)} %fusion.25.kv_ref), custom_call_target="tpu_custom_call" | custom-call | flops 4294967296 | bytes 6291456 | tf_op jit(solution)/shard_map/flash/pallas_call | solution.py:135
  44.9 1.3 collective-permute-start.3
  46.2 1.3 collective-permute-start.7
  47.5 4.2 %flash.9 = (f32[2048,128]{1,0:T(8,128)S(1)}, f32[2048,128]{1,0:T(8,128)S(1)}, f32[2048,128]{1,0:T(8,128)S(1)}) custom-call(s32[2]{0:T(128)S(1)} %pad_add_fusion.7.info_ref, f32[1]{0:T(128)} %bitcast.7.shift_ref, bf16[2048,128]{1,0:T(8,128)(2,1)S(1)} %maximum_select_fusion.q_ref, bf16[1040,256]{1,0:T(8,128)(2,1)S(1)} %collective-permute-done.2.kv_ref, ...), custom_call_target="tpu_custom_call" | custom-call | flops 4294967296 | bytes 6291456 | tf_op jit(solution)/shard_map/flash/pallas_call | solution.py:135
  51.7 6.7 %flash.10 = (f32[2048,128]{1,0:T(8,128)S(1)}, f32[2048,128]{1,0:T(8,128)S(1)}, f32[2048,128]{1,0:T(8,128)S(1)}) custom-call(s32[2]{0:T(128)S(1)} %pad_add_fusion.4.info_ref, f32[1]{0:T(128)} %bitcast.7.shift_ref, bf16[2048,128]{1,0:T(8,128)(2,1)S(1)} %maximum_select_fusion.q_ref, bf16[1040,256]{1,0:T(8,128)(2,1)S(1)} %collective-permute-done.6.kv_ref, ...), custom_call_target="tpu_custom_call" | custom-call | flops 4294967296 | bytes 6291456 | tf_op jit(solution)/shard_map/flash/pallas_call | solution.py:135
  58.4 3.4 %collective-permute-done.3.kv_ref = bf16[1040,256]{1,0:T(8,128)(2,1)S(1)} collective-permute-done((bf16[1040,256]{1,0:T(8,128)(2,1)S(1)}, bf16[1040,256]{1,0:T(8,128)(2,1)S(1)}, u32[]{:S(2)}, u32[]{:S(2)}) %collective-permute-start.3) | collective-permute-done | bytes 532512 | tf_op jit(solution)/shard_map/ppermute | solution.py:247
  61.8 1.3 collective-permute-start.4
  63.1 10.1 %collective-permute-done.7.kv_ref = bf16[1040,256]{1,0:T(8,128)(2,1)S(1)} collective-permute-done((bf16[1040,256]{1,0:T(8,128)(2,1)S(1)}, bf16[1040,256]{1,0:T(8,128)(2,1)S(1)}, u32[]{:S(2)}, u32[]{:S(2)}) %collective-permute-start.7) | collective-permute-done | bytes 532512 | tf_op jit(solution)/shard_map/ppermute | solution.py:247
  73.2 1.5 %collective-permute-start.8 = (bf16[1040,256]{1,0:T(8,128)(2,1)S(1)}, bf16[1040,256]{1,0:T(8,128)(2,1)S(1)}, u32[]{:S(2)}, u32[]{:S(2)}) collective-permute-start(bf16[1040,256]{1,0:T(8,128)(2,1)S(1)} %collective-permute-done.7.kv_ref), channel_id=1, source_target_pairs={{0,8},{4,12},{8,16},{12,20},{16,24},{20,28},{1,9},{5,13},{9,17},{1... | collective-permute-start | bytes 1597448 | tf_op jit(solution)/shard_map/ppermute | solution.py:247
  74.7 6.6 %flash.11 = (f32[2048,128]{1,0:T(8,128)S(1)}, f32[2048,128]{1,0:T(8,128)S(1)}, f32[2048,128]{1,0:T(8,128)S(1)}) custom-call(s32[2]{0:T(128)S(1)} %pad_add_fusion.5.info_ref, f32[1]{0:T(128)} %bitcast.7.shift_ref, bf16[2048,128]{1,0:T(8,128)(2,1)S(1)} %maximum_select_fusion.q_ref, bf16[1040,256]{1,0:T(8,128)(2,1)S(1)} %collective-permute-done.3.kv_ref, ...), custom_call_target="tpu_custom_call" | custom-call | flops 4294967296 | bytes 6291456 | tf_op jit(solution)/shard_map/flash/pallas_call | solution.py:135
  81.3 6.6 %flash.12 = (f32[2048,128]{1,0:T(8,128)S(1)}, f32[2048,128]{1,0:T(8,128)S(1)}, f32[2048,128]{1,0:T(8,128)S(1)}) custom-call(s32[2]{0:T(128)S(1)} %pad_add_fusion.2.info_ref, f32[1]{0:T(128)} %bitcast.7.shift_ref, bf16[2048,128]{1,0:T(8,128)(2,1)S(1)} %maximum_select_fusion.q_ref, bf16[1040,256]{1,0:T(8,128)(2,1)S(1)} %collective-permute-done.7.kv_ref, ...), custom_call_target="tpu_custom_call" | custom-call | flops 4294967296 | bytes 6291456 | tf_op jit(solution)/shard_map/flash/pallas_call | solution.py:135
  87.9 1.3 collective-permute-start.5
  89.2 6.7 %flash.13 = (f32[2048,128]{1,0:T(8,128)S(1)}, f32[2048,128]{1,0:T(8,128)S(1)}, f32[2048,128]{1,0:T(8,128)S(1)}) custom-call(s32[2]{0:T(128)S(1)} %pad_add_fusion.3.info_ref, f32[1]{0:T(128)} %bitcast.7.shift_ref, bf16[2048,128]{1,0:T(8,128)(2,1)S(1)} %maximum_select_fusion.q_ref, bf16[1040,256]{1,0:T(8,128)(2,1)S(1)} %collective-permute-done.4.kv_ref, ...), custom_call_target="tpu_custom_call" | custom-call | flops 4294967296 | bytes 6291456 | tf_op jit(solution)/shard_map/flash/pallas_call | solution.py:135
  96.0 6.6 %flash.14 = (f32[2048,128]{1,0:T(8,128)S(1)}, f32[2048,128]{1,0:T(8,128)S(1)}, f32[2048,128]{1,0:T(8,128)S(1)}) custom-call(s32[2]{0:T(128)S(1)} %pad_add_fusion.info_ref, f32[1]{0:T(128)} %bitcast.7.shift_ref, bf16[2048,128]{1,0:T(8,128)(2,1)S(1)} %maximum_select_fusion.q_ref, bf16[1040,256]{1,0:T(8,128)(2,1)S(1)} %collective-permute-done.8.kv_ref, ...), custom_call_target="tpu_custom_call" | custom-call | flops 4294967296 | bytes 6291456 | tf_op jit(solution)/shard_map/flash/pallas_call | solution.py:135
  102.6 4.3 %collective-permute-done.5.kv_ref = bf16[1040,256]{1,0:T(8,128)(2,1)S(1)} collective-permute-done((bf16[1040,256]{1,0:T(8,128)(2,1)S(1)}, bf16[1040,256]{1,0:T(8,128)(2,1)S(1)}, u32[]{:S(2)}, u32[]{:S(2)}) %collective-permute-start.5) | collective-permute-done | bytes 532512 | tf_op jit(solution)/shard_map/ppermute | solution.py:247
  106.9 7.2 %flash.15 = bf16[2048,128]{1,0:T(8,128)(2,1)} custom-call(s32[2]{0:T(128)S(1)} %pad_add_fusion.1.info_ref, f32[1]{0:T(128)} %bitcast.7.shift_ref, bf16[2048,128]{1,0:T(8,128)(2,1)S(1)} %maximum_select_fusion.q_ref, bf16[1040,256]{1,0:T(8,128)(2,1)S(1)} %collective-permute-done.5.kv_ref, f32[2048,128]{1,0:T(8,128)S(1)} %get-tuple-element.46.refs_0_, ...), custom_call_target="tpu_custom_call" | custom-call | flops 4294967296 | bytes 6291456 | tf_op jit(solution)/shard_map/flash/pallas_call | solution.py:135
  114.1 3.7 %all-to-all-start.1 = ((bf16[8,256,128]{2,1,0:T(8,128)(2,1)}), bf16[8,256,128]{2,1,0:T(8,128)(2,1)S(1)}, u32[]{:S(2)}, u32[]{:S(2)}) async-start(bf16[8,256,128]{2,1,0:T(8,128)(2,1)} %bitcast.16), calls=%async_computation.1 | async-start | bytes 1048576 | tf_op jit(solution)/shard_map/all_to_all | solution.py:339
  117.8 5.7 %convolve.1 = bf16[256,1024]{1,0:T(8,128)(2,1)S(1)} custom-call(bf16[4,384,256]{2,1,0:T(8,128)(2,1)S(1)} %all-to-all-done.window_ref), custom_call_target="tpu_custom_call" | custom-call | flops 520093696 | bytes 2097152 | tf_op jit(solution)/shard_map/convolve/pallas_call | solution.py:199
  123.5 2.9 %all-to-all-done.1 = bf16[8,256,128]{2,1,0:T(8,128)(2,1)S(1)} async-done(((bf16[8,256,128]{2,1,0:T(8,128)(2,1)}), bf16[8,256,128]{2,1,0:T(8,128)(2,1)S(1)}, u32[]{:S(2)}, u32[]{:S(2)}) %all-to-all-start.1) | async-done | bytes 524320 | tf_op jit(solution)/shard_map/all_to_all | solution.py:339
  126.6 3.5 %fusion = f32[256,2048]{1,0:T(8,128)S(1)} fusion(bf16[256,1024]{0,1:T(8,128)(2,1)S(1)} %bitcast.56, bf16[2048,2048]{1,0:T(8,128)(2,1)} %param.19), kind=kOutput, calls=%fused_computation | convolution fusion | flops 1073741824 | bytes 6815744 | tf_op jit(solution)/shard_map/dot_general | solution.py:352
  130.1 4.5 %fusion.7 = bf16[256,2048]{1,0:T(8,128)(2,1)} fusion(f32[256,2048]{1,0:T(8,128)S(1)} %fusion, bf16[256,1024]{1,0:T(8,128)(2,1)S(1)} %convolve.1, bf16[2048,2048]{1,0:T(8,128)(2,1)} %param.19), kind=kOutput, calls=%fused_computation.5 | convolution fusion | flops 1074790400 | bytes 7864320 | tf_op jit(solution)/shard_map/dot_general | solution.py:349
  (63 shorter events, 8.6 us)
Async XLA Ops:
  0.0 1.2 copy-start
  1.2 5.9 %copy-start.7 = (f32[1024,2]{0,1:T(2,128)S(1)}, f32[1024,2]{0,1:T(2,128)}, u32[]{:S(2)}) copy-start(f32[1024,2]{0,1:T(2,128)} %param.18) | copy-start | bytes 24580
  1.2 6.0 %copy-start.2 = (bf16[2048,256]{1,0:T(8,128)(2,1)S(1)}, bf16[2048,256]{1,0:T(8,128)(2,1)}, u32[]{:S(2)}) copy-start(bf16[2048,256]{1,0:T(8,128)(2,1)} %param.13) | copy-start | bytes 3145732
  1.2 6.0 %copy-start.3 = (bf16[2048,256]{1,0:T(8,128)(2,1)S(1)}, bf16[2048,256]{1,0:T(8,128)(2,1)}, u32[]{:S(2)}) copy-start(bf16[2048,256]{1,0:T(8,128)(2,1)} %param.12) | copy-start | bytes 3145732
  5.7 31.6 %collective-permute-start.1 = (bf16[1024,128]{1,0:T(8,128)(2,1)}, bf16[1024,128]{1,0:T(8,128)(2,1)}, u32[]{:S(2)}, u32[]{:S(2)}) collective-permute-start(bf16[1024,128]{1,0:T(8,128)(2,1)} %get-tuple-element.56), channel_id=1, source_target_pairs={{0,4},{4,0},{8,12},{12,8},{16,20},{20,16},{24,28},{28,24},{1,5},{5... | collective-permute-start | bytes 786440 | tf_op jit(solution)/shard_map/ppermute | solution.py:244
  7.3 2.6 %copy-start.9 = (bf16[1024,2048]{1,0:T(8,128)(2,1)S(1)}, bf16[1024,2048]{1,0:T(8,128)(2,1)}, u32[]{:S(2)}) copy-start(bf16[1024,2048]{1,0:T(8,128)(2,1)} %param.10) | copy-start | bytes 12582916
  9.8 2.7 %copy-start.4 = (bf16[2048,128]{1,0:T(8,128)(2,1)S(1)}, bf16[2048,128]{1,0:T(8,128)(2,1)}, u32[]{:S(2)}) copy-start(bf16[2048,128]{1,0:T(8,128)(2,1)} %get-tuple-element.53) | copy-start | bytes 1572868
  9.8 2.7 %copy-start.5 = (bf16[2048,128]{1,0:T(8,128)(2,1)S(1)}, bf16[2048,128]{1,0:T(8,128)(2,1)}, u32[]{:S(2)}) copy-start(bf16[2048,128]{1,0:T(8,128)(2,1)} %get-tuple-element.67) | copy-start | bytes 1572868
  11.9 33.0 %collective-permute-start.2 = (bf16[1040,256]{1,0:T(8,128)(2,1)}, bf16[1040,256]{1,0:T(8,128)(2,1)S(1)}, u32[]{:S(2)}, u32[]{:S(2)}) collective-permute-start(bf16[1040,256]{1,0:T(8,128)(2,1)} %fusion.24), channel_id=1, source_target_pairs={{0,4},{4,0},{8,12},{12,8},{16,20},{20,16},{24,28},{28,24},{1,5},{5... | collective-permute-start | bytes 1597448 | tf_op jit(solution)/shard_map/ppermute | solution.py:244
  12.5 5.1 %copy-start.10 = (bf16[1024,2048]{1,0:T(8,128)(2,1)S(1)}, bf16[1024,2048]{1,0:T(8,128)(2,1)}, u32[]{:S(2)}) copy-start(bf16[1024,2048]{1,0:T(8,128)(2,1)} %param.10) | copy-start | bytes 12582916
  12.5 5.1 %copy-start.11 = (bf16[2048,256]{1,0:T(8,128)(2,1)S(1)}, bf16[2048,256]{1,0:T(8,128)(2,1)}, u32[]{:S(2)}) copy-start(bf16[2048,256]{1,0:T(8,128)(2,1)} %param.15) | copy-start | bytes 3145732
  16.2 2.7 %copy-start.12 = (bf16[2048,256]{1,0:T(8,128)(2,1)S(1)}, bf16[2048,256]{1,0:T(8,128)(2,1)}, u32[]{:S(2)}) copy-start(bf16[2048,256]{1,0:T(8,128)(2,1)} %param.14) | copy-start | bytes 3145732
  16.2 30.0 %collective-permute-start.6 = (bf16[1040,256]{1,0:T(8,128)(2,1)S(1)}, bf16[1040,256]{1,0:T(8,128)(2,1)S(1)}, u32[]{:S(2)}, u32[]{:S(2)}) collective-permute-start(bf16[1040,256]{1,0:T(8,128)(2,1)S(1)} %fusion.25.kv_ref), channel_id=1, source_target_pairs={{0,8},{4,12},{8,16},{12,20},{16,24},{20,28},{1,9},{5,13},{9,17},{1... | collective-permute-start | bytes 1597448 | tf_op jit(solution)/shard_map/ppermute | solution.py:247
  18.9 5.3 %copy-start.6 = (f32[31,256]{1,0:T(8,128)S(1)}, f32[31,256]{1,0:T(8,128)}, u32[]{:S(2)}) copy-start(f32[31,256]{1,0:T(8,128)} %param.16) | copy-start | bytes 95236
  18.9 5.3 %copy-start.8 = (f32[256]{0:T(256)S(1)}, f32[256]{0:T(256)}, u32[]{:S(2)}) copy-start(f32[256]{0:T(256)} %param.17) | copy-start | bytes 3076
  20.2 12.6 %collective-permute-start = (bf16[32,256]{1,0:T(8,128)(2,1)S(1)}, bf16[32,256]{1,0:T(8,128)(2,1)S(1)}, u32[]{:S(2)}, u32[]{:S(2)}) collective-permute-start(bf16[32,256]{1,0:T(8,128)(2,1)S(1)} %slice.32), channel_id=1, source_target_pairs={{0,4},{4,8},{8,12},{12,16},{16,20},{20,24},{24,28},{1,5},{5,9},{9,... | collective-permute-start | bytes 49160 | tf_op jit(solution)/shard_map/ppermute | solution.py:287
  32.9 0.9 copy-start.1
  33.8 80.3 %all-to-all-start = ((bf16[4,384,256]{2,1,0:T(8,128)(2,1)}), bf16[4,384,256]{2,1,0:T(8,128)(2,1)S(1)}, u32[]{:S(2)}, u32[]{:S(2)}) async-start(bf16[4,384,256]{2,1,0:T(8,128)(2,1)} %bitcast.55), calls=%async_computation | async-start | bytes 1572864 | tf_op jit(solution)/shard_map/all_to_all | solution.py:296
  44.9 16.9 %collective-permute-start.3 = (bf16[1040,256]{1,0:T(8,128)(2,1)S(1)}, bf16[1040,256]{1,0:T(8,128)(2,1)S(1)}, u32[]{:S(2)}, u32[]{:S(2)}) collective-permute-start(bf16[1040,256]{1,0:T(8,128)(2,1)S(1)} %collective-permute-done.2.kv_ref), channel_id=1, source_target_pairs={{0,8},{4,12},{8,16},{12,20},{16,24},{20,28},{1,9},{5,13},{9,17},{1... | collective-permute-start | bytes 1597448 | tf_op jit(solution)/shard_map/ppermute | solution.py:247
  46.2 27.0 %collective-permute-start.7 = (bf16[1040,256]{1,0:T(8,128)(2,1)S(1)}, bf16[1040,256]{1,0:T(8,128)(2,1)S(1)}, u32[]{:S(2)}, u32[]{:S(2)}) collective-permute-start(bf16[1040,256]{1,0:T(8,128)(2,1)S(1)} %collective-permute-done.6.kv_ref), channel_id=1, source_target_pairs={{0,8},{4,12},{8,16},{12,20},{16,24},{20,28},{1,9},{5,13},{9,17},{1... | collective-permute-start | bytes 1597448 | tf_op jit(solution)/shard_map/ppermute | solution.py:247
  61.8 26.1 %collective-permute-start.4 = (bf16[1040,256]{1,0:T(8,128)(2,1)S(1)}, bf16[1040,256]{1,0:T(8,128)(2,1)S(1)}, u32[]{:S(2)}, u32[]{:S(2)}) collective-permute-start(bf16[1040,256]{1,0:T(8,128)(2,1)S(1)} %collective-permute-done.3.kv_ref), channel_id=1, source_target_pairs={{0,8},{4,12},{8,16},{12,20},{16,24},{20,28},{1,9},{5,13},{9,17},{1... | collective-permute-start | bytes 1597448 | tf_op jit(solution)/shard_map/ppermute | solution.py:247
  73.2 22.8 %collective-permute-start.8 = (bf16[1040,256]{1,0:T(8,128)(2,1)S(1)}, bf16[1040,256]{1,0:T(8,128)(2,1)S(1)}, u32[]{:S(2)}, u32[]{:S(2)}) collective-permute-start(bf16[1040,256]{1,0:T(8,128)(2,1)S(1)} %collective-permute-done.7.kv_ref), channel_id=1, source_target_pairs={{0,8},{4,12},{8,16},{12,20},{16,24},{20,28},{1,9},{5,13},{9,17},{1... | collective-permute-start | bytes 1597448 | tf_op jit(solution)/shard_map/ppermute | solution.py:247
  87.9 19.1 %collective-permute-start.5 = (bf16[1040,256]{1,0:T(8,128)(2,1)S(1)}, bf16[1040,256]{1,0:T(8,128)(2,1)S(1)}, u32[]{:S(2)}, u32[]{:S(2)}) collective-permute-start(bf16[1040,256]{1,0:T(8,128)(2,1)S(1)} %collective-permute-done.4.kv_ref), channel_id=1, source_target_pairs={{0,8},{4,12},{8,16},{12,20},{16,24},{20,28},{1,9},{5,13},{9,17},{1... | collective-permute-start | bytes 1597448 | tf_op jit(solution)/shard_map/ppermute | solution.py:247
  114.1 12.3 %all-to-all-start.1 = ((bf16[8,256,128]{2,1,0:T(8,128)(2,1)}), bf16[8,256,128]{2,1,0:T(8,128)(2,1)S(1)}, u32[]{:S(2)}, u32[]{:S(2)}) async-start(bf16[8,256,128]{2,1,0:T(8,128)(2,1)} %bitcast.16), calls=%async_computation.1 | async-start | bytes 1048576 | tf_op jit(solution)/shard_map/all_to_all | solution.py:339

commit v3 on v2

--- a/solution.py
+++ b/solution.py
@@ -195,7 +195,7 @@
 
 
 def convolve(windows, *, taps, halo, rows, total_channels):
-    groups, depth, channels = windows.shape
+    groups, _, channels = windows.shape
     return pl.pallas_call(
         functools.partial(
             conv_body, taps=taps, halo=halo, rows=rows, total_channels=total_channels
@@ -210,7 +210,7 @@
     )(windows)
 
 
-def on_device(
+def layer(
     inputs,
     w_query,
     w_key,
@@ -269,10 +269,13 @@
     else:
         kv_own, gates_own = keys_and_values(place)
         halves = [kv_own]
+    inputs, kv_own = lax.optimization_barrier((inputs, kv_own))
+    halves[0] = kv_own
     query_rows = jnp.dot(inputs, w_query, preferred_element_type=f32).astype(jnp.bfloat16)
     q = columns_of(query_rows, place, width)
     if group == 2:
-        q_partner = swap(columns_of(query_rows, 1 - place, width))
+        q_other = columns_of(query_rows, 1 - place, width)
+        q_partner = swap(q_other)
         q = jnp.where(
             place == 0,
             jnp.concatenate([q, q_partner], axis=0),
@@ -293,7 +296,8 @@
     pieces = []
     for t in range(tp_count):
         pieces += [padded[t * out_rows : t * out_rows + out_rows + halo], table]
-    windows = lax.all_to_all(jnp.concatenate(pieces, axis=0), "tp", 0, 0, tiled=True)
+    pieces = jnp.concatenate(pieces, axis=0)
+    windows = lax.all_to_all(pieces, "tp", 0, 0, tiled=True)
     windows = windows.reshape(tp_count, -1, channels)
 
     tile = min(512, tok_rows)
@@ -321,7 +325,9 @@
     for number in range(blocks):
         ready = halves
         if number < blocks - 1:
-            halves = [hop(half) for half in ready]
+            halves = []
+            for half in ready:
+                halves.append(hop(half))
         for part, half in enumerate(ready):
             finished = number == blocks - 1 and part == len(ready) - 1
             valid = (block >= number).astype(jnp.int32)
@@ -346,11 +352,9 @@
     conv_rows = convolve(
         windows, taps=kernel, halo=halo, rows=out_rows, total_channels=total_channels
     )
-    projected = jnp.dot(conv_rows, w_out[:total_channels], preferred_element_type=f32)
     attn = jnp.transpose(attn, (2, 1, 0, 3)).reshape(out_rows, -1)
-    return (
-        projected + jnp.dot(attn, w_out[total_channels:], preferred_element_type=f32)
-    ).astype(jnp.bfloat16)
+    both = jnp.concatenate([conv_rows, attn], axis=1)
+    return jnp.dot(both, w_out, preferred_element_type=f32).astype(jnp.bfloat16)
 
 
 def solution(mesh):
@@ -368,5 +372,5 @@
     )
     out_specs = P(("sp", "tp"), None)
     return jax.shard_map(
-        on_device, mesh=mesh, in_specs=in_specs, out_specs=out_specs, check_vma=False
+        layer, mesh=mesh, in_specs=in_specs, out_specs=out_specs, check_vma=False
     )

time: 135 us -> 132 us (0.978)
  matrix products: 18.9 us -> 15.3 us
    dot_general x5 -> x4, matrix products: 14 us -> 10.5 us  [the longest x1 6.68 us: layer(): return jnp.dot(both, w_out, preferred_element_type=f32).astype(jnp.bfloat16)]
    unnamed x32 -> x24, local copies, waits for them, and re-layouts: 3.42 us -> 1.96 us
  transfers between devices with their start and end apart: 11 -> 11, of which waited for: 6 -> 6; matrix products, arithmetic and copies ran while one was open for 9% -> 7% of each run, Pallas kernels for 42% -> 43%
where the time goes in v3:
time: 132 us; the launch traced here: 131 us
  Pallas kernels  56.3 us (43%)
  waiting for transfers between devices  28.8 us (22%)
  starting transfers between devices  20.5 us (16%)
  matrix products  15.3 us (12%)
  local copies, waits for them, and re-layouts  6.15 us (5%)
  other arithmetic  3.71 us (3%)
    pallas_call x8, Pallas kernels, flash(): pl.pallas_call(functools.partial(flash_body, heads=heads, rows=rows, sub=...  50.6 us
    ppermute x6, waiting for transfers between devices, hop(): lax.ppermute(value, 'sp', [(i, i + group) for i in range(sp_count - group)])  18.1 us
    ppermute x6, starting transfers between devices, hop(): lax.ppermute(value, 'sp', [(i, i + group) for i in range(sp_count - group)])  7.9 us
    ppermute x1, waiting for transfers between devices, layer(): lax.ppermute(gated[tok_rows - halo:], 'sp', [(i, i + 1) for i in range(sp...  7.86 us
    dot_general x1, matrix products, layer(): return jnp.dot(both, w_out, preferred_element_type=f32).astype(jnp.bfloat16)  6.68 us
    pallas_call x1, Pallas kernels, convolve(): pl.pallas_call(functools.partial(conv_body, taps=taps, halo=halo, rows=ro...  5.69 us
    dot_general x2, matrix products, keys_and_values(): jnp.dot(inputs, weight, preferred_element_type=f32).astype(jnp.bfloat16)  4.83 us
    all_to_all x1, starting transfers between devices, layer(): lax.all_to_all(attn, ('sp', 'tp'), 0, 0, axis_index_groups=members, tiled...  3.71 us
  transfers between devices with their start and end apart: 11, of which 6 were waited for; matrix products, arithmetic and copies ran while one was open for 7% of the time, Pallas kernels for 43%

profile of v3, /device:TPU:24, one launch (start us, length us, event | category | flops | bytes accessed | tf_op | source)
XLA Modules:
  0.0 131.3 jit_solution(3371456628811109011)
XLA Ops:
  0.9 1.8 %constant_dynamic-slice_fusion.1 = (bf16[2048,128]{1,0:T(8,128)(2,1)S(1)}, bf16[2048,128]{1,0:T(8,128)(2,1)S(1)}, bf16[2048,128]{1,0:T(8,128)(2,1)S(1)}, bf16[2048,128]{1,0:T(8,128)(2,1)S(1)}) fusion(bf16[2048,256]{1,0:T(8,128)(2,1)} %param.13, s32[]{:T(128)S(6)} %select_n.33, s32[]{:T(128)S(6)} %select_n.29, bf16[2048,256]{1,0:T(8,128)(2,1)} %param.12), kind=kLoop, calls=%fused_computation.56 | loop fusion | bytes 4194312 | tf_op jit(solution)/shard_map/dynamic_slice | solution.py:252
  3.7 1.2 fusion.4
  5.0 1.3 convolution_convert_fusion.3
  7.1 1.5 %collective-permute-start.1 = (bf16[1024,128]{1,0:T(8,128)(2,1)}, bf16[1024,128]{1,0:T(8,128)(2,1)}, u32[]{:S(2)}, u32[]{:S(2)}) collective-permute-start(bf16[1024,128]{1,0:T(8,128)(2,1)} %get-tuple-element.60), channel_id=1, source_target_pairs={{0,4},{4,0},{8,12},{12,8},{16,20},{20,16},{24,28},{28,24},{1,5},{5... | collective-permute-start | bytes 786440 | tf_op jit(solution)/shard_map/ppermute | solution.py:244
  8.7 3.6 %fusion.5 = bf16[1024,256]{1,0:T(8,128)(2,1)S(1)} fusion(bf16[1024,2048]{1,0:T(8,128)(2,1)} %param.10, bf16[2048,128]{1,0:T(8,128)(2,1)S(1)} %get-tuple-element.57, bf16[2048,128]{1,0:T(8,128)(2,1)S(1)} %get-tuple-element.73), kind=kOutput, calls=%fused_computation.11 | convolution fusion | flops 1076101120 | bytes 5767168 | tf_op jit(solution)/shard_map/dot_general | solution.py:258
  13.6 1.3 collective-permute-start.6
  14.9 1.3 fusion.2
  16.3 1.2 fusion.3
  17.5 3.4 %collective-permute-start = (bf16[32,256]{1,0:T(8,128)(2,1)S(1)}, bf16[32,256]{1,0:T(8,128)(2,1)S(1)}, u32[]{:S(2)}, u32[]{:S(2)}) collective-permute-start(bf16[32,256]{1,0:T(8,128)(2,1)S(1)} %slice.24), channel_id=1, source_target_pairs={{0,4},{4,8},{8,12},{12,16},{16,20},{20,24},{24,28},{1,5},{5,9},{9,... | collective-permute-start | bytes 49160 | tf_op jit(solution)/shard_map/ppermute | solution.py:290
  22.2 7.9 %collective-permute-done = bf16[32,256]{1,0:T(8,128)(2,1)S(1)} collective-permute-done((bf16[32,256]{1,0:T(8,128)(2,1)S(1)}, bf16[32,256]{1,0:T(8,128)(2,1)S(1)}, u32[]{:S(2)}, u32[]{:S(2)}) %collective-permute-start) | collective-permute-done | bytes 16416 | tf_op jit(solution)/shard_map/ppermute | solution.py:290
  31.1 3.5 %all-to-all-start = ((bf16[4,384,256]{2,1,0:T(8,128)(2,1)}), bf16[4,384,256]{2,1,0:T(8,128)(2,1)S(1)}, u32[]{:S(2)}, u32[]{:S(2)}) async-start(bf16[4,384,256]{2,1,0:T(8,128)(2,1)} %bitcast.53), calls=%async_computation | async-start | bytes 1572864 | tf_op jit(solution)/shard_map/all_to_all | solution.py:300
  34.6 1.3 %maximum_select_fusion.q_ref = bf16[2048,128]{1,0:T(8,128)(2,1)S(1)} fusion(bf16[1024,128]{1,0:T(8,128)(2,1)} %collective-permute-done.1, bf16[1024,128]{1,0:T(8,128)(2,1)} %get-tuple-element.59, pred[]{:T(512)S(6)} %eq.3), kind=kLoop, calls=%fused_computation.26 | loop fusion | flops 2359296 | bytes 1048577 | tf_op jit(solution)/shard_map/jit(_where)/select_n | solution.py:279
  35.9 6.2 %flash.8 = (f32[2048,128]{1,0:T(8,128)S(1)}, f32[2048,128]{1,0:T(8,128)S(1)}, f32[2048,128]{1,0:T(8,128)S(1)}) custom-call(s32[2]{0:T(128)S(1)} %pad_add_fusion.6.info_ref, f32[1]{0:T(128)} %bitcast.9.shift_ref, bf16[2048,128]{1,0:T(8,128)(2,1)S(1)} %maximum_select_fusion.q_ref, bf16[1040,256]{1,0:T(8,128)(2,1)S(1)} %fusion.17.kv_ref), custom_call_target="tpu_custom_call" | custom-call | flops 4294967296 | bytes 6291456 | tf_op jit(solution)/shard_map/flash/pallas_call | solution.py:135
  42.1 1.3 collective-permute-start.3
  43.4 1.3 collective-permute-start.7
  44.7 4.2 %flash.9 = (f32[2048,128]{1,0:T(8,128)S(1)}, f32[2048,128]{1,0:T(8,128)S(1)}, f32[2048,128]{1,0:T(8,128)S(1)}) custom-call(s32[2]{0:T(128)S(1)} %pad_add_fusion.7.info_ref, f32[1]{0:T(128)} %bitcast.9.shift_ref, bf16[2048,128]{1,0:T(8,128)(2,1)S(1)} %maximum_select_fusion.q_ref, bf16[1040,256]{1,0:T(8,128)(2,1)S(1)} %collective-permute-done.2.kv_ref, ...), custom_call_target="tpu_custom_call" | custom-call | flops 4294967296 | bytes 6291456 | tf_op jit(solution)/shard_map/flash/pallas_call | solution.py:135
  48.9 6.7 %flash.10 = (f32[2048,128]{1,0:T(8,128)S(1)}, f32[2048,128]{1,0:T(8,128)S(1)}, f32[2048,128]{1,0:T(8,128)S(1)}) custom-call(s32[2]{0:T(128)S(1)} %pad_add_fusion.4.info_ref, f32[1]{0:T(128)} %bitcast.9.shift_ref, bf16[2048,128]{1,0:T(8,128)(2,1)S(1)} %maximum_select_fusion.q_ref, bf16[1040,256]{1,0:T(8,128)(2,1)S(1)} %collective-permute-done.6.kv_ref, ...), custom_call_target="tpu_custom_call" | custom-call | flops 4294967296 | bytes 6291456 | tf_op jit(solution)/shard_map/flash/pallas_call | solution.py:135
  55.6 3.4 %collective-permute-done.3.kv_ref = bf16[1040,256]{1,0:T(8,128)(2,1)S(1)} collective-permute-done((bf16[1040,256]{1,0:T(8,128)(2,1)S(1)}, bf16[1040,256]{1,0:T(8,128)(2,1)S(1)}, u32[]{:S(2)}, u32[]{:S(2)}) %collective-permute-start.3) | collective-permute-done | bytes 532512 | tf_op jit(solution)/shard_map/ppermute | solution.py:247
  59.0 1.3 collective-permute-start.4
  60.3 10.1 %collective-permute-done.7.kv_ref = bf16[1040,256]{1,0:T(8,128)(2,1)S(1)} collective-permute-done((bf16[1040,256]{1,0:T(8,128)(2,1)S(1)}, bf16[1040,256]{1,0:T(8,128)(2,1)S(1)}, u32[]{:S(2)}, u32[]{:S(2)}) %collective-permute-start.7) | collective-permute-done | bytes 532512 | tf_op jit(solution)/shard_map/ppermute | solution.py:247
  70.4 1.5 %collective-permute-start.8 = (bf16[1040,256]{1,0:T(8,128)(2,1)S(1)}, bf16[1040,256]{1,0:T(8,128)(2,1)S(1)}, u32[]{:S(2)}, u32[]{:S(2)}) collective-permute-start(bf16[1040,256]{1,0:T(8,128)(2,1)S(1)} %collective-permute-done.7.kv_ref), channel_id=1, source_target_pairs={{0,8},{4,12},{8,16},{12,20},{16,24},{20,28},{1,9},{5,13},{9,17},{1... | collective-permute-start | bytes 1597448 | tf_op jit(solution)/shard_map/ppermute | solution.py:247
  71.9 6.7 %flash.11 = (f32[2048,128]{1,0:T(8,128)S(1)}, f32[2048,128]{1,0:T(8,128)S(1)}, f32[2048,128]{1,0:T(8,128)S(1)}) custom-call(s32[2]{0:T(128)S(1)} %pad_add_fusion.5.info_ref, f32[1]{0:T(128)} %bitcast.9.shift_ref, bf16[2048,128]{1,0:T(8,128)(2,1)S(1)} %maximum_select_fusion.q_ref, bf16[1040,256]{1,0:T(8,128)(2,1)S(1)} %collective-permute-done.3.kv_ref, ...), custom_call_target="tpu_custom_call" | custom-call | flops 4294967296 | bytes 6291456 | tf_op jit(solution)/shard_map/flash/pallas_call | solution.py:135
  78.6 6.6 %flash.12 = (f32[2048,128]{1,0:T(8,128)S(1)}, f32[2048,128]{1,0:T(8,128)S(1)}, f32[2048,128]{1,0:T(8,128)S(1)}) custom-call(s32[2]{0:T(128)S(1)} %pad_add_fusion.2.info_ref, f32[1]{0:T(128)} %bitcast.9.shift_ref, bf16[2048,128]{1,0:T(8,128)(2,1)S(1)} %maximum_select_fusion.q_ref, bf16[1040,256]{1,0:T(8,128)(2,1)S(1)} %collective-permute-done.7.kv_ref, ...), custom_call_target="tpu_custom_call" | custom-call | flops 4294967296 | bytes 6291456 | tf_op jit(solution)/shard_map/flash/pallas_call | solution.py:135
  85.1 1.3 collective-permute-start.5
  86.4 6.6 %flash.13 = (f32[2048,128]{1,0:T(8,128)S(1)}, f32[2048,128]{1,0:T(8,128)S(1)}, f32[2048,128]{1,0:T(8,128)S(1)}) custom-call(s32[2]{0:T(128)S(1)} %pad_add_fusion.3.info_ref, f32[1]{0:T(128)} %bitcast.9.shift_ref, bf16[2048,128]{1,0:T(8,128)(2,1)S(1)} %maximum_select_fusion.q_ref, bf16[1040,256]{1,0:T(8,128)(2,1)S(1)} %collective-permute-done.4.kv_ref, ...), custom_call_target="tpu_custom_call" | custom-call | flops 4294967296 | bytes 6291456 | tf_op jit(solution)/shard_map/flash/pallas_call | solution.py:135
  93.2 6.6 %flash.14 = (f32[2048,128]{1,0:T(8,128)S(1)}, f32[2048,128]{1,0:T(8,128)S(1)}, f32[2048,128]{1,0:T(8,128)S(1)}) custom-call(s32[2]{0:T(128)S(1)} %pad_add_fusion.info_ref, f32[1]{0:T(128)} %bitcast.9.shift_ref, bf16[2048,128]{1,0:T(8,128)(2,1)S(1)} %maximum_select_fusion.q_ref, bf16[1040,256]{1,0:T(8,128)(2,1)S(1)} %collective-permute-done.8.kv_ref, ...), custom_call_target="tpu_custom_call" | custom-call | flops 4294967296 | bytes 6291456 | tf_op jit(solution)/shard_map/flash/pallas_call | solution.py:135
  99.8 4.3 %collective-permute-done.5.kv_ref = bf16[1040,256]{1,0:T(8,128)(2,1)S(1)} collective-permute-done((bf16[1040,256]{1,0:T(8,128)(2,1)S(1)}, bf16[1040,256]{1,0:T(8,128)(2,1)S(1)}, u32[]{:S(2)}, u32[]{:S(2)}) %collective-permute-start.5) | collective-permute-done | bytes 532512 | tf_op jit(solution)/shard_map/ppermute | solution.py:247
  104.1 7.2 %flash.15 = bf16[2048,128]{1,0:T(8,128)(2,1)} custom-call(s32[2]{0:T(128)S(1)} %pad_add_fusion.1.info_ref, f32[1]{0:T(128)} %bitcast.9.shift_ref, bf16[2048,128]{1,0:T(8,128)(2,1)S(1)} %maximum_select_fusion.q_ref, bf16[1040,256]{1,0:T(8,128)(2,1)S(1)} %collective-permute-done.5.kv_ref, f32[2048,128]{1,0:T(8,128)S(1)} %get-tuple-element.50.refs_0_, ...), custom_call_target="tpu_custom_call" | custom-call | flops 4294967296 | bytes 6291456 | tf_op jit(solution)/shard_map/flash/pallas_call | solution.py:135
  111.4 3.7 %all-to-all-start.1 = ((bf16[8,256,128]{2,1,0:T(8,128)(2,1)}), bf16[8,256,128]{2,1,0:T(8,128)(2,1)S(1)}, u32[]{:S(2)}, u32[]{:S(2)}) async-start(bf16[8,256,128]{2,1,0:T(8,128)(2,1)} %bitcast.16), calls=%async_computation.1 | async-start | bytes 1048576 | tf_op jit(solution)/shard_map/all_to_all | solution.py:345
  115.1 5.7 %convolve.1 = bf16[256,1024]{1,0:T(8,128)(2,1)S(1)} custom-call(bf16[4,384,256]{2,1,0:T(8,128)(2,1)S(1)} %all-to-all-done.window_ref), custom_call_target="tpu_custom_call" | custom-call | flops 520093696 | bytes 2097152 | tf_op jit(solution)/shard_map/convolve/pallas_call | solution.py:199
  120.8 2.9 %all-to-all-done.1 = bf16[8,256,128]{2,1,0:T(8,128)(2,1)S(1)} async-done(((bf16[8,256,128]{2,1,0:T(8,128)(2,1)}), bf16[8,256,128]{2,1,0:T(8,128)(2,1)S(1)}, u32[]{:S(2)}, u32[]{:S(2)}) %all-to-all-start.1) | async-done | bytes 524320 | tf_op jit(solution)/shard_map/all_to_all | solution.py:345
  124.6 6.7 %convolution_convert_fusion = bf16[256,2048]{1,0:T(8,128)(2,1)} fusion(bf16[2048,2048]{1,0:T(8,128)(2,1)} %param.19, bf16[256,1024]{1,0:T(8,128)(2,1)S(1)} %reshape.249, bf16[256,1024]{1,0:T(8,128)(2,1)S(1)} %convolve.1), kind=kOutput, calls=%fused_computation | convolution fusion | flops 2150105088 | bytes 10485760 | tf_op jit(solution)/shard_map/dot_general | solution.py:357
  (55 shorter events, 7.5 us)
Async XLA Ops:
  0.0 5.0 %copy-start = (bf16[2048,256]{1,0:T(8,128)(2,1)S(1)}, bf16[2048,256]{1,0:T(8,128)(2,1)}, u32[]{:S(2)}) copy-start(bf16[2048,256]{1,0:T(8,128)(2,1)} %param.11) | copy-start | bytes 3145732
  0.9 2.8 %copy-start.5 = (bf16[1024,2048]{1,0:T(8,128)(2,1)S(1)}, bf16[1024,2048]{1,0:T(8,128)(2,1)}, u32[]{:S(2)}) copy-start(bf16[1024,2048]{1,0:T(8,128)(2,1)} %param.10) | copy-start | bytes 12582916
  7.1 27.5 %collective-permute-start.1 = (bf16[1024,128]{1,0:T(8,128)(2,1)}, bf16[1024,128]{1,0:T(8,128)(2,1)}, u32[]{:S(2)}, u32[]{:S(2)}) collective-permute-start(bf16[1024,128]{1,0:T(8,128)(2,1)} %get-tuple-element.60), channel_id=1, source_target_pairs={{0,4},{4,0},{8,12},{12,8},{16,20},{20,16},{24,28},{28,24},{1,5},{5... | collective-permute-start | bytes 786440 | tf_op jit(solution)/shard_map/ppermute | solution.py:244
  8.7 6.3 %copy-start.6 = (bf16[1024,2048]{1,0:T(8,128)(2,1)S(1)}, bf16[1024,2048]{1,0:T(8,128)(2,1)}, u32[]{:S(2)}) copy-start(bf16[1024,2048]{1,0:T(8,128)(2,1)} %param.10) | copy-start | bytes 12582916
  8.7 6.3 %copy-start.7 = (bf16[2048,256]{1,0:T(8,128)(2,1)S(1)}, bf16[2048,256]{1,0:T(8,128)(2,1)}, u32[]{:S(2)}) copy-start(bf16[2048,256]{1,0:T(8,128)(2,1)} %param.15) | copy-start | bytes 3145732
  13.1 3.1 %copy-start.8 = (bf16[2048,256]{1,0:T(8,128)(2,1)S(1)}, bf16[2048,256]{1,0:T(8,128)(2,1)}, u32[]{:S(2)}) copy-start(bf16[2048,256]{1,0:T(8,128)(2,1)} %param.14) | copy-start | bytes 3145732
  13.1 29.0 %collective-permute-start.2 = (bf16[1040,256]{1,0:T(8,128)(2,1)}, bf16[1040,256]{1,0:T(8,128)(2,1)S(1)}, u32[]{:S(2)}, u32[]{:S(2)}) collective-permute-start(bf16[1040,256]{1,0:T(8,128)(2,1)} %fusion.18), channel_id=1, source_target_pairs={{0,4},{4,0},{8,12},{12,8},{16,20},{20,16},{24,28},{28,24},{1,5},{5... | collective-permute-start | bytes 1597448 | tf_op jit(solution)/shard_map/ppermute | solution.py:244
  13.6 29.8 %collective-permute-start.6 = (bf16[1040,256]{1,0:T(8,128)(2,1)S(1)}, bf16[1040,256]{1,0:T(8,128)(2,1)S(1)}, u32[]{:S(2)}, u32[]{:S(2)}) collective-permute-start(bf16[1040,256]{1,0:T(8,128)(2,1)S(1)} %fusion.17.kv_ref), channel_id=1, source_target_pairs={{0,8},{4,12},{8,16},{12,20},{16,24},{20,28},{1,9},{5,13},{9,17},{1... | collective-permute-start | bytes 1597448 | tf_op jit(solution)/shard_map/ppermute | solution.py:247
  16.2 4.7 %copy-start.3 = (f32[1024,2]{0,1:T(2,128)S(1)}, f32[1024,2]{0,1:T(2,128)}, u32[]{:S(2)}) copy-start(f32[1024,2]{0,1:T(2,128)} %param.18) | copy-start | bytes 24580
  16.2 5.3 %copy-start.2 = (f32[31,256]{1,0:T(8,128)S(1)}, f32[31,256]{1,0:T(8,128)}, u32[]{:S(2)}) copy-start(f32[31,256]{1,0:T(8,128)} %param.16) | copy-start | bytes 95236
  16.3 5.3 %copy-start.4 = (f32[256]{0:T(256)S(1)}, f32[256]{0:T(256)}, u32[]{:S(2)}) copy-start(f32[256]{0:T(256)} %param.17) | copy-start | bytes 3076
  17.5 12.5 %collective-permute-start = (bf16[32,256]{1,0:T(8,128)(2,1)S(1)}, bf16[32,256]{1,0:T(8,128)(2,1)S(1)}, u32[]{:S(2)}, u32[]{:S(2)}) collective-permute-start(bf16[32,256]{1,0:T(8,128)(2,1)S(1)} %slice.24), channel_id=1, source_target_pairs={{0,4},{4,8},{8,12},{12,16},{16,20},{20,24},{24,28},{1,5},{5,9},{9,... | collective-permute-start | bytes 49160 | tf_op jit(solution)/shard_map/ppermute | solution.py:290
  30.2 0.9 copy-start.1
  31.1 80.3 %all-to-all-start = ((bf16[4,384,256]{2,1,0:T(8,128)(2,1)}), bf16[4,384,256]{2,1,0:T(8,128)(2,1)S(1)}, u32[]{:S(2)}, u32[]{:S(2)}) async-start(bf16[4,384,256]{2,1,0:T(8,128)(2,1)} %bitcast.53), calls=%async_computation | async-start | bytes 1572864 | tf_op jit(solution)/shard_map/all_to_all | solution.py:300
  42.1 16.9 %collective-permute-start.3 = (bf16[1040,256]{1,0:T(8,128)(2,1)S(1)}, bf16[1040,256]{1,0:T(8,128)(2,1)S(1)}, u32[]{:S(2)}, u32[]{:S(2)}) collective-permute-start(bf16[1040,256]{1,0:T(8,128)(2,1)S(1)} %collective-permute-done.2.kv_ref), channel_id=1, source_target_pairs={{0,8},{4,12},{8,16},{12,20},{16,24},{20,28},{1,9},{5,13},{9,17},{1... | collective-permute-start | bytes 1597448 | tf_op jit(solution)/shard_map/ppermute | solution.py:247
  43.4 27.0 %collective-permute-start.7 = (bf16[1040,256]{1,0:T(8,128)(2,1)S(1)}, bf16[1040,256]{1,0:T(8,128)(2,1)S(1)}, u32[]{:S(2)}, u32[]{:S(2)}) collective-permute-start(bf16[1040,256]{1,0:T(8,128)(2,1)S(1)} %collective-permute-done.6.kv_ref), channel_id=1, source_target_pairs={{0,8},{4,12},{8,16},{12,20},{16,24},{20,28},{1,9},{5,13},{9,17},{1... | collective-permute-start | bytes 1597448 | tf_op jit(solution)/shard_map/ppermute | solution.py:247
  59.0 26.1 %collective-permute-start.4 = (bf16[1040,256]{1,0:T(8,128)(2,1)S(1)}, bf16[1040,256]{1,0:T(8,128)(2,1)S(1)}, u32[]{:S(2)}, u32[]{:S(2)}) collective-permute-start(bf16[1040,256]{1,0:T(8,128)(2,1)S(1)} %collective-permute-done.3.kv_ref), channel_id=1, source_target_pairs={{0,8},{4,12},{8,16},{12,20},{16,24},{20,28},{1,9},{5,13},{9,17},{1... | collective-permute-start | bytes 1597448 | tf_op jit(solution)/shard_map/ppermute | solution.py:247
  70.4 22.8 %collective-permute-start.8 = (bf16[1040,256]{1,0:T(8,128)(2,1)S(1)}, bf16[1040,256]{1,0:T(8,128)(2,1)S(1)}, u32[]{:S(2)}, u32[]{:S(2)}) collective-permute-start(bf16[1040,256]{1,0:T(8,128)(2,1)S(1)} %collective-permute-done.7.kv_ref), channel_id=1, source_target_pairs={{0,8},{4,12},{8,16},{12,20},{16,24},{20,28},{1,9},{5,13},{9,17},{1... | collective-permute-start | bytes 1597448 | tf_op jit(solution)/shard_map/ppermute | solution.py:247
  85.1 19.0 %collective-permute-start.5 = (bf16[1040,256]{1,0:T(8,128)(2,1)S(1)}, bf16[1040,256]{1,0:T(8,128)(2,1)S(1)}, u32[]{:S(2)}, u32[]{:S(2)}) collective-permute-start(bf16[1040,256]{1,0:T(8,128)(2,1)S(1)} %collective-permute-done.4.kv_ref), channel_id=1, source_target_pairs={{0,8},{4,12},{8,16},{12,20},{16,24},{20,28},{1,9},{5,13},{9,17},{1... | collective-permute-start | bytes 1597448 | tf_op jit(solution)/shard_map/ppermute | solution.py:247
  111.4 12.3 %all-to-all-start.1 = ((bf16[8,256,128]{2,1,0:T(8,128)(2,1)}), bf16[8,256,128]{2,1,0:T(8,128)(2,1)S(1)}, u32[]{:S(2)}, u32[]{:S(2)}) async-start(bf16[8,256,128]{2,1,0:T(8,128)(2,1)} %bitcast.16), calls=%async_computation.1 | async-start | bytes 1048576 | tf_op jit(solution)/shard_map/all_to_all | solution.py:345
